TPU v7x, 32 devices: a whole 2x2x4 slice. The times are simulated.
32 devices in a mesh: sp: 8 (over z, y), tp: 4 (over x, core).
Axes of the slice: x: 2, y: 2, z: 4, core: 2. Of those that a mesh axis runs over, the one named last changes fastest.
Arguments:
- pooled_in: bfloat16 [8192, 2048], P('sp', 'tp'), may hold values from -6 to 6
- group_map: bfloat16 [4, 512, 512], P('tp'), may hold values from -0.25 to 0.25
- pool_scale: float32 [2048], P('tp'), may hold values from 0.1 to 1.9
- out_weight: bfloat16 [2048, 2048], P('tp'), may hold values from -0.125 to 0.125
- residual: bfloat16 [8192, 2048], P(('sp', 'tp')), may hold values from -6 to 6
- norm_gain: float32 [2048], replicated, may hold values from 0.1 to 1.9
- gate_weight: bfloat16 [8, 2048, 512], P('sp'), may hold values from -0.125 to 0.125
- up_weight: bfloat16 [8, 2048, 512], P('sp'), may hold values from -0.125 to 0.125
- down_weight: bfloat16 [8, 512, 2048], P('sp'), may hold values from -0.25 to 0.25
- route_expert: int32 [8192, 2], P(('sp', 'tp')), may hold values from 0 to 7, all different within a row; in each aligned block of 256 rows (0 to 255, 256 to 511, ...) at most 96 rows name the same one
- route_score: float32 [8192, 2], P(('sp', 'tp')), may hold values from 0.05 to 1
Outputs:
- layer_out: bfloat16 [8192, 2048], P(('sp', 'tp'))
Inputs may be any that keep to these rules, and one draw needn't show every extreme that they name: `route_expert`: each token names 2 different experts. Within each aligned block of 256 tokens (the rows of one device) no expert is named by more than 96 tokens, and in some such block one expert is named by exactly 96.
All inputs are finite; a program needn't handle non-finite values.
Results may differ from a plain program's by a relative error of at most 0.0065.
Values may be sent and summed in bfloat16 or wider, within the bound.
No kernel may reach another device: no remote copies, remote signals or barrier semaphores. Data moves between devices by JAX's collectives and lax.ppermute only.
A program may use at most 64 MiB of HBM per device.

v0:
```python
import functools

import jax
import jax.numpy as jnp
from jax import lax
from jax.experimental import pallas as pl
from jax.experimental.pallas import tpu as pltpu
from jax.sharding import PartitionSpec as P


HALO = 16
CHUNKS = 2

f32 = jnp.float32
bf16 = jnp.bfloat16

VMEM = pl.BlockSpec(memory_space=pltpu.VMEM)
SMEM = pl.BlockSpec(memory_space=pltpu.SMEM)
ANY = pl.BlockSpec(memory_space=pl.ANY)


def dot(a, b):
    return jnp.dot(a, b, preferred_element_type=f32)


def crossed(value, axis, partner):
    peers = lax.axis_size(axis)
    return lax.ppermute(value, axis, [(i, partner(i)) for i in range(peers)])


def flipped(value, axis, bits):
    return crossed(value, axis, lambda i: i ^ bits)


def reversed_pairs(count):
    return lambda i: (count - 2 - (i // 2) * 2) + i % 2


def pool_kernel(at_ref, halo_ref, x_ref, map_ref, scale_ref, *rest):
    out_refs = rest
    blocks = len(out_refs)
    rows = x_ref.shape[0] // blocks
    window = at_ref[0]
    behind = lax.broadcasted_iota(jnp.int32, (rows, rows), 0) - lax.broadcasted_iota(
        jnp.int32, (rows, rows), 1
    )
    band = jnp.where((behind >= 0) & (behind < window), 1.0, 0.0).astype(bf16)
    early = (
        HALO
        + lax.broadcasted_iota(jnp.int32, (HALO, HALO), 0)
        - lax.broadcasted_iota(jnp.int32, (HALO, HALO), 1)
    )
    early_band = jnp.where(early < window, 1.0, 0.0).astype(bf16)
    for k in [*range(1, blocks, 2), *range(0, blocks, 2)]:
        block = at_ref[2] ^ k
        x = x_ref[pl.ds(pl.multiple_of(block * rows, rows), rows), :]
        before = pl.multiple_of(jnp.maximum(block * rows - HALO, 0), HALO)
        tail = jnp.where(block == 0, halo_ref[...], x_ref[pl.ds(before, HALO), :])
        sums = dot(band, x)
        sums = jnp.concatenate([sums[:HALO] + dot(early_band, tail), sums[HALO:]], axis=0)
        position = at_ref[1] + block * rows + lax.broadcasted_iota(jnp.int32, (rows, 1), 0)
        share = 1.0 / jnp.minimum(position + 1, window).astype(f32)
        contrast = (sums * share - x.astype(f32)).astype(bf16)
        out_refs[k][...] = (dot(contrast, map_ref[0]) * scale_ref[...]).astype(bf16)


def pooled_blocks(pooled_in, group_map, pool_scale):
    rows, width = pooled_in.shape
    replicas = lax.axis_size("tp")
    peers = lax.axis_size("sp")
    halo = lax.ppermute(
        pooled_in[rows - HALO :], "sp", [(i, i + 1) for i in range(peers - 1)]
    )
    tp_at = lax.axis_index("tp")
    at = jnp.stack([jnp.left_shift(jnp.int32(2), tp_at), lax.axis_index("sp") * rows, tp_at])
    return pl.pallas_call(
        pool_kernel,
        in_specs=[SMEM, VMEM, VMEM, VMEM, VMEM],
        out_specs=[VMEM] * replicas,
        out_shape=[jax.ShapeDtypeStruct((rows // replicas, width), bf16)] * replicas,
        name="pool",
    )(at.astype(jnp.int32), halo, pooled_in, group_map, pool_scale[None, :])


def project_kernel(count, *refs):
    mine = refs[:count]
    mates = refs[count : 2 * count]
    w_mine, w_mate, residual = refs[2 * count : 2 * count + 3]
    outs = refs[2 * count + 3 : -1]
    lines = refs[-1]
    rows, width = mine[0].shape

    @pl.when(pl.program_id(0) == 0)
    def _():
        for n in range(count):
            lines[n * rows : (n + 1) * rows, :width] = mine[n][...]
            lines[n * rows : (n + 1) * rows, width:] = mates[n][...]

    sums = dot(lines[:, :width], w_mine[...]) + dot(lines[:, width:], w_mate[...])
    outs[0][...] = sums[:rows] + residual[...].astype(f32)
    for n in range(1, count):
        outs[n][...] = sums[n * rows : (n + 1) * rows].astype(bf16)


def projections(mine, mates, w_mine, w_mate, residual, chunk, columns):
    count = len(mine)
    rows, width = mine[0].shape
    step = min(512, columns)
    steps = columns // step
    whole = pl.BlockSpec((rows, width), lambda j: (0, 0))
    weight = pl.BlockSpec((width, step), lambda j: (0, chunk * steps + j))
    tile = pl.BlockSpec((rows, step), lambda j: (0, j))
    return pl.pallas_call(
        functools.partial(project_kernel, count),
        grid=(steps,),
        in_specs=[whole] * (2 * count)
        + [weight, weight, pl.BlockSpec((rows, step), lambda j: (0, chunk * steps + j))],
        out_specs=[tile] * count,
        out_shape=[jax.ShapeDtypeStruct((rows, columns), f32)]
        + [jax.ShapeDtypeStruct((rows, columns), bf16)] * (count - 1),
        scratch_shapes=[pltpu.VMEM((count * rows, 2 * width), bf16)],
        name="project",
    )(*mine, *mates, w_mine, w_mate, residual)


def send_kernel(others, slots_ref, own_ref, *refs):
    parts = refs[:others]
    middle_ref = refs[others]
    outs = refs[others + 1 :]
    total = own_ref[...]
    for part in parts:
        total = total + part[...].astype(f32)
    middle = total.astype(bf16)
    middle_ref[...] = middle
    length = outs[0].shape[0]
    rows = own_ref.shape[0]
    for k, out in enumerate(outs):
        slot = k * length + lax.broadcasted_iota(jnp.int32, (length, rows), 0)
        hit = slot == slots_ref[0:1, :]
        for j in range(1, slots_ref.shape[0]):
            hit = hit | (slot == slots_ref[j : j + 1, :])
        out[...] = dot(jnp.where(hit, 1.0, 0.0).astype(bf16), middle).astype(bf16)


def rows_to_send(slots_t, own, parts, group, length):
    rows, columns = own.shape
    return pl.pallas_call(
        functools.partial(send_kernel, len(parts)),
        in_specs=[VMEM] * (2 + len(parts)),
        out_specs=[VMEM] * (1 + group),
        out_shape=[jax.ShapeDtypeStruct((rows, columns), bf16)]
        + [jax.ShapeDtypeStruct((length, columns), bf16)] * group,
        name="send",
    )(slots_t, own, *parts)


def expert_kernel(group, chunks, swapped, pieces, at_ref, gain_ref, *refs):
    row_refs = refs[: group * chunks]
    refs = refs[group * chunks :]
    weights = refs[: 2 * pieces if swapped else 3]
    refs = refs[len(weights) :]
    outs = refs[:group]
    lines, gate_up, down, sems = refs[group:]
    capacity = outs[0].shape[0]
    part = lines.shape[1] // pieces
    hidden_units = gate_up.shape[3]

    def copies(k):
        if swapped:
            both, out = weights[2 * k], weights[2 * k + 1]
            return (
                pltpu.make_async_copy(both.at[0:part, :], gate_up.at[k, 0], sems.at[k, 0]),
                pltpu.make_async_copy(
                    both.at[part : 2 * part, :], gate_up.at[k, 1], sems.at[k, 1]
                ),
                pltpu.make_async_copy(out, down.at[k], sems.at[k, 2]),
            )
        gate, up, out = weights
        span = pl.ds(k * part, part)
        return (
            pltpu.make_async_copy(gate.at[0, span, :], gate_up.at[k, 0], sems.at[k, 0]),
            pltpu.make_async_copy(up.at[0, span, :], gate_up.at[k, 1], sems.at[k, 1]),
            pltpu.make_async_copy(out.at[0, :, span], down.at[k], sems.at[k, 2]),
        )

    moves = [copies(k) for k in range(pieces)]
    for k in range(pieces):
        moves[k][0].start()
        moves[k][1].start()
    for k in range(pieces):
        moves[k][2].start()
    for p in range(group):
        blocks = [row_refs[p * chunks + c][...].astype(f32) for c in range(chunks)]
        square = sum(jnp.sum(b * b, axis=1, keepdims=True) for b in blocks)
        factor = lax.rsqrt(square / lines.shape[1] + 1e-06)
        at = 0
        for b in blocks:
            span = slice(at, at + b.shape[1])
            lines[p * capacity : (p + 1) * capacity, span] = (
                b * factor * gain_ref[:, span]
            ).astype(bf16)
            at += b.shape[1]

    def offset(k):
        if swapped:
            return pl.multiple_of((at_ref[0] ^ k) * part, part)
        return k * part

    gate_part = jnp.zeros((group * capacity, hidden_units), f32)
    up_part = jnp.zeros((group * capacity, hidden_units), f32)
    for k in range(pieces):
        moves[k][0].wait()
        moves[k][1].wait()
        x = lines[:, pl.ds(offset(k), part)]
        gate_part = gate_part + dot(x, gate_up[k, 0])
        up_part = up_part + dot(x, gate_up[k, 1])
    hidden = (gate_part / (1.0 + jnp.exp(-gate_part)) * up_part).astype(bf16)
    for k in range(pieces):
        moves[k][2].wait()
        made = dot(hidden, down[k]).astype(bf16)
        for p in range(group):
            outs[p][:, pl.ds(offset(k), part)] = made[p * capacity : (p + 1) * capacity]


def expert(row_blocks, side, norm_gain, weights, swapped):
    group = len(row_blocks)
    chunks = len(row_blocks[0])
    capacity = row_blocks[0][0].shape[0] // 2
    pieces = lax.axis_size("tp")
    width = norm_gain.shape[0]
    hidden_units = weights[0].shape[-1]
    part = width // pieces
    flat = [b for blocks in row_blocks for b in blocks]
    return pl.pallas_call(
        functools.partial(expert_kernel, group, chunks, swapped, pieces),
        grid=(1,),
        in_specs=[SMEM, pl.BlockSpec((1, width), lambda i: (0, 0))]
        + [pl.BlockSpec((capacity, b.shape[1]), lambda i: (side, 0)) for b in flat]
        + [ANY] * len(weights),
        out_specs=[pl.BlockSpec((capacity, width), lambda i: (0, 0))] * group,
        out_shape=[jax.ShapeDtypeStruct((capacity, width), bf16)] * group,
        scratch_shapes=[
            pltpu.VMEM((group * capacity, width), bf16),
            pltpu.VMEM((pieces, 2, part, hidden_units), bf16),
            pltpu.VMEM((pieces, hidden_units, part), bf16),
            pltpu.SemaphoreType.DMA((pieces, 3)),
        ],
        name="expert_swapped" if swapped else "expert_own",
    )(lax.axis_index("tp")[None], norm_gain[None, :], *flat, *weights)


def combine_kernel(group, side, slots_ref, share_ref, *refs):
    row_refs = refs[:group]
    base_refs = refs[group:-2]
    out_ref, back = refs[-2:]
    capacity = row_refs[0].shape[0]
    rows = out_ref.shape[0]
    for p in range(group):
        back[p * capacity : (p + 1) * capacity, :] = row_refs[p][...]
    column = lax.broadcasted_iota(jnp.int32, (rows, group * capacity), 1)
    peer = sum((column >= p * capacity).astype(jnp.int32) for p in range(1, group))
    slot = column + (peer + side) * capacity
    weigh = jnp.zeros((rows, group * capacity), f32)
    for j in range(slots_ref.shape[1]):
        weigh = weigh + jnp.where(slot == slots_ref[:, j : j + 1], share_ref[:, j : j + 1], 0.0)
    high = weigh.astype(bf16)
    low = (weigh - high.astype(f32)).astype(bf16)
    at = 0
    for base in base_refs:
        span = slice(at, at + base.shape[1])
        total = base[...].astype(f32) + dot(high, back[:, span]) + dot(low, back[:, span])
        out_ref[:, span] = total.astype(out_ref.dtype)
        at += base.shape[1]


def combined(slots, shares, bases, returned, side, dtype):
    group = len(returned)
    capacity, width = returned[0].shape
    steps = 4 if len(bases) == 1 else 1
    tile = lambda v: pl.BlockSpec((v.shape[0], v.shape[1] // steps), lambda j: (0, j))
    small = pl.BlockSpec(slots.shape, lambda j: (0, 0))
    out = jax.ShapeDtypeStruct((slots.shape[0], width), dtype)
    return pl.pallas_call(
        functools.partial(combine_kernel, group, side),
        grid=(steps,),
        in_specs=[small, small] + [tile(v) for v in [*returned, *bases]],
        out_specs=tile(out),
        out_shape=out,
        scratch_shapes=[pltpu.VMEM((group * capacity, width // steps), bf16)],
        name="combine",
    )(slots, shares, *returned, *bases)


def body(
    pooled_in,
    group_map,
    pool_scale,
    out_weight,
    residual,
    norm_gain,
    gate_weight,
    up_weight,
    down_weight,
    route_expert,
    route_score,
):
    experts = lax.axis_size("sp")
    replicas = lax.axis_size("tp")
    sp_at = lax.axis_index("sp")
    tp_at = lax.axis_index("tp")
    rows, width = residual.shape
    top = route_expert.shape[1]
    capacity = max(2, 3 * rows * top // (2 * experts))
    capacity = -(-capacity // 16) * 16
    group = experts // 2
    other_half = reversed_pairs(experts)
    columns = width // CHUNKS

    part = width // replicas
    start = tp_at * part
    gate_up = jnp.concatenate(
        [
            lax.dynamic_slice_in_dim(gate_weight[0], start, part, 0),
            lax.dynamic_slice_in_dim(up_weight[0], start, part, 0),
        ],
        axis=0,
    )
    down = lax.dynamic_slice_in_dim(down_weight[0], start, part, 1)
    far = [(0, crossed(gate_up, "sp", other_half), crossed(down, "sp", other_half))]

    here = jnp.arange(experts, dtype=jnp.int32)
    owner = jnp.where(here // group == sp_at // group, here, other_half(here))
    block_of = 2 * (owner ^ sp_at) + (owner != here).astype(jnp.int32)
    named = route_expert[:, :, None] == here[None, None, :]
    hits = jnp.any(named, axis=1)
    earlier = jnp.arange(rows)[:, None] > jnp.arange(rows)[None, :]
    rank = dot(earlier.astype(bf16), hits.astype(bf16)).astype(jnp.int32)
    slot_of = block_of[None, :] * capacity + rank
    slots = jnp.sum(jnp.where(named, slot_of[:, None, :], 0), axis=2)
    slots_t = slots.T
    shares = route_score / jnp.sum(route_score, axis=1, keepdims=True)

    mate_weight = flipped(out_weight, "tp", 1)
    pooled = pooled_blocks(pooled_in, group_map, pool_scale)
    mine = pooled[0::2]
    mates = [flipped(v, "tp", 1) for v in pooled[1::2]]
    sums = []
    for c in range(CHUNKS):
        sums.append(projections(mine, mates, out_weight, mate_weight, residual, c, columns))
    middles = []
    arrived = [[] for _ in range(group)]
    for c in range(CHUNKS):
        own, *leaving = sums[c]
        parts = [flipped(v, "tp", 2 * (n + 1)) for n, v in enumerate(leaving)]
        middle, *outgoing = rows_to_send(slots_t, own, parts, group, 2 * capacity)
        middles.append(middle)
        arrived[0].append(outgoing[0])
        for k in range(1, group):
            arrived[k].append(flipped(outgoing[k], "sp", k))
    bit = replicas // 2
    while bit:
        far = far + [
            (k ^ bit, flipped(v, "tp", bit), flipped(w, "tp", bit))
            for k, v, w in far
        ]
        bit //= 2
    far.sort(key=lambda entry: entry[0])
    far_weights = [v for entry in far for v in entry[1:]]

    def sent_back(made):
        return [made[0]] + [flipped(made[k], "sp", k) for k in range(1, group)]

    made = expert(arrived, 0, norm_gain, (gate_weight, up_weight, down_weight), False)
    back = sent_back(made)
    made = expert(arrived, 1, norm_gain, far_weights, True)
    far_back = sent_back(made)
    total = combined(slots, shares, middles, back, 0, f32)
    return combined(slots, shares, [total], far_back, 1, bf16)


def solution(mesh):
    in_specs = (
        P("sp", "tp"),
        P("tp", None, None),
        P("tp"),
        P("tp", None),
        P(("sp", "tp"), None),
        P(),
        P("sp", None, None),
        P("sp", None, None),
        P("sp", None, None),
        P(("sp", "tp"), None),
        P(("sp", "tp"), None),
    )
    out_specs = P(("sp", "tp"), None)
    return jax.shard_map(body, mesh=mesh, in_specs=in_specs, out_specs=out_specs, check_vma=False)
```

profile of v0, /device:TPU:0, one launch (start us, length us, event | category | flops | bytes accessed | tf_op | source)
XLA Modules:
  0.0 208.2 jit_solution(13653472780012826094)
XLA Ops:
  0.5 1.3 dynamic-slice_bitcast_fusion.1
  1.8 1.0 pad_maximum_fusion
  2.8 4.6 %collective-permute-start.12 = (bf16[1024,512]{1,0:T(8,128)(2,1)}, bf16[1024,512]{1,0:T(8,128)(2,1)}, u32[]{:S(2)}, u32[]{:S(2)}) collective-permute-start(bf16[1024,512]{1,0:T(8,128)(2,1)} %pad_maximum_fusion), channel_id=1, source_target_pairs={{0,24},{4,28},{8,16},{12,20},{16,8},{20,12},{24,0},{28,4},{1,25},{... | collective-permute-start | bytes 3145736 | tf_op jit(solution)/shard_map/ppermute | solution.py:28
  7.4 0.7 slice.3
  8.1 3.4 %collective-permute-start = (bf16[16,512]{1,0:T(8,128)(2,1)S(1)}, bf16[16,512]{1,0:T(8,128)(2,1)S(1)}, u32[]{:S(2)}, u32[]{:S(2)}) collective-permute-start(bf16[16,512]{1,0:T(8,128)(2,1)S(1)} %slice.3), channel_id=1, source_target_pairs={{0,4},{4,8},{8,12},{12,16},{16,20},{20,24},{24,28},{1,5},{5,9},{9,... | collective-permute-start | bytes 49160 | tf_op jit(solution)/shard_map/ppermute | solution.py:71
  11.5 1.9 dynamic-slice_bitcast_fusion
  14.9 3.6 %pool.1 = (bf16[256,512]{1,0:T(8,128)(2,1)}, bf16[256,512]{1,0:T(8,128)(2,1)}, bf16[256,512]{1,0:T(8,128)(2,1)}, bf16[256,512]{1,0:T(8,128)(2,1)}) custom-call(s32[3]{0:T(128)} %pad_add_fusion.at_ref, bf16[16,512]{1,0:T(8,128)(2,1)} %copy-done.20, bf16[1024,512]{1,0:T(8,128)(2,1)} %x_ref.1, bf16[1,512,512]{2,1,0:T(8,128)(2,1)} %map_ref.1, f32[1,512]{1,0:T(1,128)} %bitcast.17), custom_call_target="tpu_custom_call" | custom-call | tf_op jit(solution)/shard_map/pool/pallas_call | solution.py:76
  19.0 12.8 %collective-permute-done.12.refs_8_ = bf16[1024,512]{1,0:T(8,128)(2,1)} collective-permute-done((bf16[1024,512]{1,0:T(8,128)(2,1)}, bf16[1024,512]{1,0:T(8,128)(2,1)}, u32[]{:S(2)}, u32[]{:S(2)}) %collective-permute-start.12) | collective-permute-done | bytes 1048608 | tf_op jit(solution)/shard_map/ppermute | solution.py:28
  31.8 1.7 collective-permute-start.16
  33.6 0.7 copy-done.7
  34.4 0.6 copy-done
  35.0 4.1 %project.2 = (f32[256,1024]{1,0:T(8,128)}, bf16[256,1024]{1,0:T(8,128)(2,1)}) custom-call(bf16[256,512]{1,0:T(8,128)(2,1)} %get-tuple-element.31.refs_0_, bf16[256,512]{1,0:T(8,128)(2,1)} %get-tuple-element.32.refs_1_, bf16[256,512]{1,0:T(8,128)(2,1)} %copy-done.7, bf16[256,512]{1,0:T(8,128)(2,1)} %copy-done.8, bf16[512,2048]{1,0:T(8,128)(2,1)} %refs_4_.3, ...), custom_call_target="tpu_custom_call" | custom-call | tf_op jit(solution)/shard_map/project/pallas_call | solution.py:113
  39.5 4.2 %project.3 = (f32[256,1024]{1,0:T(8,128)}, bf16[256,1024]{1,0:T(8,128)(2,1)}) custom-call(bf16[256,512]{1,0:T(8,128)(2,1)} %get-tuple-element.31.refs_0_, bf16[256,512]{1,0:T(8,128)(2,1)} %get-tuple-element.32.refs_1_, bf16[256,512]{1,0:T(8,128)(2,1)} %copy-done.7, bf16[256,512]{1,0:T(8,128)(2,1)} %copy-done.8, bf16[512,2048]{1,0:T(8,128)(2,1)} %refs_4_.3, ...), custom_call_target="tpu_custom_call" | custom-call | tf_op jit(solution)/shard_map/project/pallas_call | solution.py:113
  43.7 1.7 collective-permute-start.5
  46.0 0.6 select_reduce_fusion
  46.6 22.7 %collective-permute-done.4.refs_0_ = bf16[256,1024]{1,0:T(8,128)(2,1)S(1)} collective-permute-done((bf16[256,1024]{1,0:T(8,128)(2,1)}, bf16[256,1024]{1,0:T(8,128)(2,1)S(1)}, u32[]{:S(2)}, u32[]{:S(2)}) %collective-permute-start.4) | collective-permute-done | bytes 524320 | tf_op jit(solution)/shard_map/ppermute | solution.py:28
  69.3 0.8 copy-done.12
  70.1 2.9 %send.2 = (bf16[256,1024]{1,0:T(8,128)(2,1)}, bf16[192,1024]{1,0:T(8,128)(2,1)}, bf16[192,1024]{1,0:T(8,128)(2,1)}, bf16[192,1024]{1,0:T(8,128)(2,1)}, bf16[192,1024]{1,0:T(8,128)(2,1)}) custom-call(s32[2,256]{1,0:T(2,128)} %bitcast.13, f32[256,1024]{1,0:T(8,128)} %get-tuple-element.35.own_ref, bf16[256,1024]{1,0:T(8,128)(2,1)} %copy-done.12), custom_call_target="tpu_custom_call" | custom-call | tf_op jit(solution)/shard_map/send/pallas_call | solution.py:147
  73.0 6.1 %collective-permute-start.6 = (bf16[192,1024]{1,0:T(8,128)(2,1)}, bf16[192,1024]{1,0:T(8,128)(2,1)S(1)}, u32[]{:S(2)}, u32[]{:S(2)}) collective-permute-start(bf16[192,1024]{1,0:T(8,128)(2,1)} %get-tuple-element.41), channel_id=1, source_target_pairs={{0,4},{4,0},{8,12},{12,8},{16,20},{20,16},{24,28},{28,24},{1,5},{5... | collective-permute-start | bytes 1179656 | tf_op jit(solution)/shard_map/ppermute | solution.py:28
  79.0 1.5 collective-permute-done.5.refs_0_
  80.5 0.8 copy-done.11
  81.3 2.8 %send.3 = (bf16[256,1024]{1,0:T(8,128)(2,1)}, bf16[192,1024]{1,0:T(8,128)(2,1)}, bf16[192,1024]{1,0:T(8,128)(2,1)}, bf16[192,1024]{1,0:T(8,128)(2,1)}, bf16[192,1024]{1,0:T(8,128)(2,1)}) custom-call(s32[2,256]{1,0:T(2,128)} %bitcast.14, f32[256,1024]{1,0:T(8,128)} %get-tuple-element.38.own_ref, bf16[256,1024]{1,0:T(8,128)(2,1)} %copy-done.11), custom_call_target="tpu_custom_call" | custom-call | tf_op jit(solution)/shard_map/send/pallas_call | solution.py:147
  84.2 6.1 %collective-permute-start.7 = (bf16[192,1024]{1,0:T(8,128)(2,1)}, bf16[192,1024]{1,0:T(8,128)(2,1)S(1)}, u32[]{:S(2)}, u32[]{:S(2)}) collective-permute-start(bf16[192,1024]{1,0:T(8,128)(2,1)} %get-tuple-element.42), channel_id=1, source_target_pairs={{0,4},{4,0},{8,12},{12,8},{16,20},{20,16},{24,28},{28,24},{1,5},{5... | collective-permute-start | bytes 1179656 | tf_op jit(solution)/shard_map/ppermute | solution.py:28
  90.2 33.2 %collective-permute-start.8 = (bf16[192,1024]{1,0:T(8,128)(2,1)}, bf16[192,1024]{1,0:T(8,128)(2,1)S(1)}, u32[]{:S(2)}, u32[]{:S(2)}) collective-permute-start(bf16[192,1024]{1,0:T(8,128)(2,1)} %get-tuple-element.43), channel_id=1, source_target_pairs={{0,8},{4,12},{8,0},{12,4},{16,24},{20,28},{24,16},{28,20},{1,9},{5... | collective-permute-start | bytes 1179656 | tf_op jit(solution)/shard_map/ppermute | solution.py:28
  124.2 8.0 %collective-permute-start.10 = (bf16[192,1024]{1,0:T(8,128)(2,1)}, bf16[192,1024]{1,0:T(8,128)(2,1)S(1)}, u32[]{:S(2)}, u32[]{:S(2)}) collective-permute-start(bf16[192,1024]{1,0:T(8,128)(2,1)} %get-tuple-element.45), channel_id=1, source_target_pairs={{0,12},{4,8},{8,4},{12,0},{16,28},{20,24},{24,20},{28,16},{1,13},{... | collective-permute-start | bytes 1179656 | tf_op jit(solution)/shard_map/ppermute | solution.py:28
  132.3 1.3 collective-permute-done.8.refs_4_
  133.6 8.4 %collective-permute-done.9.refs_5_ = bf16[192,1024]{1,0:T(8,128)(2,1)S(1)} collective-permute-done((bf16[192,1024]{1,0:T(8,128)(2,1)}, bf16[192,1024]{1,0:T(8,128)(2,1)S(1)}, u32[]{:S(2)}, u32[]{:S(2)}) %collective-permute-start.9) | collective-permute-done | bytes 393248 | tf_op jit(solution)/shard_map/ppermute | solution.py:28
  142.0 8.1 %collective-permute-done.10.refs_6_ = bf16[192,1024]{1,0:T(8,128)(2,1)S(1)} collective-permute-done((bf16[192,1024]{1,0:T(8,128)(2,1)}, bf16[192,1024]{1,0:T(8,128)(2,1)S(1)}, u32[]{:S(2)}, u32[]{:S(2)}) %collective-permute-start.10) | collective-permute-done | bytes 393248 | tf_op jit(solution)/shard_map/ppermute | solution.py:28
  150.1 6.4 %collective-permute-done.11.refs_7_ = bf16[192,1024]{1,0:T(8,128)(2,1)S(1)} collective-permute-done((bf16[192,1024]{1,0:T(8,128)(2,1)}, bf16[192,1024]{1,0:T(8,128)(2,1)S(1)}, u32[]{:S(2)}, u32[]{:S(2)}) %collective-permute-start.11) | collective-permute-done | bytes 393248 | tf_op jit(solution)/shard_map/ppermute | solution.py:28
  156.5 0.7 copy-done.6
  157.3 7.6 %expert_own.1 = (bf16[96,2048]{1,0:T(8,128)(2,1)}, bf16[96,2048]{1,0:T(8,128)(2,1)}, bf16[96,2048]{1,0:T(8,128)(2,1)}, bf16[96,2048]{1,0:T(8,128)(2,1)}) custom-call(s32[1]{0:T(128)} %bitcast.at_ref, f32[1,2048]{1,0:T(1,128)} %bitcast.15, bf16[192,1024]{1,0:T(8,128)(2,1)} %get-tuple-element.37.refs_0_, bf16[192,1024]{1,0:T(8,128)(2,1)} %get-tuple-element.40.refs_1_, ...), custom_call_target="tpu_custom_call" | custom-call | tf_op jit(solution)/shard_map/expert_own/pallas_call | solution.py:234
  164.9 1.1 collective-permute-start.23
  166.0 1.7 collective-permute-start.24
  167.7 0.7 collective-permute-start.25
  168.4 1.0 copy-done.9
  169.4 7.7 %expert_swapped.1 = (bf16[96,2048]{1,0:T(8,128)(2,1)}, bf16[96,2048]{1,0:T(8,128)(2,1)}, bf16[96,2048]{1,0:T(8,128)(2,1)}, bf16[96,2048]{1,0:T(8,128)(2,1)}) custom-call(s32[1]{0:T(128)} %bitcast.at_ref, f32[1,2048]{1,0:T(1,128)} %bitcast.16, bf16[192,1024]{1,0:T(8,128)(2,1)} %get-tuple-element.37.refs_0_, bf16[192,1024]{1,0:T(8,128)(2,1)} %get-tuple-element.40.refs_1_, ...), custom_call_target="tpu_custom_call" | custom-call | tf_op jit(solution)/shard_map/expert_swapped/pallas_call | solution.py:234
  177.1 1.1 collective-permute-start.20
  178.2 1.7 collective-permute-start.21
  179.9 0.7 collective-permute-start.22
  180.6 0.8 copy.19.slots_ref
  181.6 0.8 broadcast_divide_fusion.share_ref
  182.4 4.7 %collective-permute-done.25.refs_3_ = bf16[96,2048]{1,0:T(8,128)(2,1)S(1)} collective-permute-done((bf16[96,2048]{1,0:T(8,128)(2,1)}, bf16[96,2048]{1,0:T(8,128)(2,1)S(1)}, u32[]{:S(2)}, u32[]{:S(2)}) %collective-permute-start.25) | collective-permute-done | bytes 393248 | tf_op jit(solution)/shard_map/ppermute | solution.py:28
  187.1 0.8 copy-done.15
  187.9 4.6 %combine.2.refs_4_ = f32[256,2048]{1,0:T(8,128)} custom-call(s32[256,2]{1,0:T(8,128)} %copy.19.slots_ref, f32[256,2]{1,0:T(8,128)} %broadcast_divide_fusion.share_ref, bf16[96,2048]{1,0:T(8,128)(2,1)} %get-tuple-element.51.refs_0_, bf16[96,2048]{1,0:T(8,128)(2,1)} %copy-done.13, bf16[96,2048]{1,0:T(8,128)(2,1)} %copy-done.14, bf16[96,2048]{1,0:T(8,128)(2,1)} %copy-done.15, ...), custom_call_target="tpu_custom_call" | custom-call | tf_op jit(solution)/shard_map/combine/pallas_call | solution.py:283
  192.4 3.0 %collective-permute-done.20.refs_1_ = bf16[96,2048]{1,0:T(8,128)(2,1)S(1)} collective-permute-done((bf16[96,2048]{1,0:T(8,128)(2,1)}, bf16[96,2048]{1,0:T(8,128)(2,1)S(1)}, u32[]{:S(2)}, u32[]{:S(2)}) %collective-permute-start.20) | collective-permute-done | bytes 393248 | tf_op jit(solution)/shard_map/ppermute | solution.py:28
  195.4 6.8 %collective-permute-done.22.refs_3_ = bf16[96,2048]{1,0:T(8,128)(2,1)S(1)} collective-permute-done((bf16[96,2048]{1,0:T(8,128)(2,1)}, bf16[96,2048]{1,0:T(8,128)(2,1)S(1)}, u32[]{:S(2)}, u32[]{:S(2)}) %collective-permute-start.22) | collective-permute-done | bytes 393248 | tf_op jit(solution)/shard_map/ppermute | solution.py:28
  202.2 0.7 copy-done.18
  202.9 5.3 %combine.3 = bf16[256,2048]{1,0:T(8,128)(2,1)} custom-call(s32[256,2]{1,0:T(8,128)} %copy.19.slots_ref, f32[256,2]{1,0:T(8,128)} %broadcast_divide_fusion.share_ref, bf16[96,2048]{1,0:T(8,128)(2,1)} %get-tuple-element.47.refs_0_, bf16[96,2048]{1,0:T(8,128)(2,1)} %copy-done.16, bf16[96,2048]{1,0:T(8,128)(2,1)} %copy-done.17, bf16[96,2048]{1,0:T(8,128)(2,1)} %copy-done.18, ...), custom_call_target="tpu_custom_call" | custom-call | tf_op jit(solution)/shard_map/combine/pallas_call | solution.py:283
  (72 shorter events, 4.5 us)
Async XLA Ops:
  0.0 33.6 %collective-permute-start.3 = (bf16[512,2048]{1,0:T(8,128)(2,1)}, bf16[512,2048]{1,0:T(8,128)(2,1)S(1)}, u32[]{:S(2)}, u32[]{:S(2)}) collective-permute-start(bf16[512,2048]{1,0:T(8,128)(2,1)} %refs_4_.3), channel_id=1, source_target_pairs={{0,1},{1,0},{2,3},{3,2},{4,5},{5,4},{6,7},{7,6},{8,9},{9,8},{10,11... | collective-permute-start | bytes 6291464 | tf_op jit(solution)/shard_map/ppermute | solution.py:28
  2.8 29.0 %collective-permute-start.12 = (bf16[1024,512]{1,0:T(8,128)(2,1)}, bf16[1024,512]{1,0:T(8,128)(2,1)}, u32[]{:S(2)}, u32[]{:S(2)}) collective-permute-start(bf16[1024,512]{1,0:T(8,128)(2,1)} %pad_maximum_fusion), channel_id=1, source_target_pairs={{0,24},{4,28},{8,16},{12,20},{16,8},{20,12},{24,0},{28,4},{1,25},{... | collective-permute-start | bytes 3145736 | tf_op jit(solution)/shard_map/ppermute | solution.py:28
  8.1 6.1 %collective-permute-start = (bf16[16,512]{1,0:T(8,128)(2,1)S(1)}, bf16[16,512]{1,0:T(8,128)(2,1)S(1)}, u32[]{:S(2)}, u32[]{:S(2)}) collective-permute-start(bf16[16,512]{1,0:T(8,128)(2,1)S(1)} %slice.3), channel_id=1, source_target_pairs={{0,4},{4,8},{8,12},{12,16},{16,20},{20,24},{24,28},{1,5},{5,9},{9,... | collective-permute-start | bytes 49160 | tf_op jit(solution)/shard_map/ppermute | solution.py:71
  13.4 32.0 %collective-permute-start.13 = (bf16[512,512]{1,0:T(8,128)(2,1)}, bf16[512,512]{1,0:T(8,128)(2,1)S(1)}, u32[]{:S(2)}, u32[]{:S(2)}) collective-permute-start(bf16[512,512]{1,0:T(8,128)(2,1)} %dynamic-slice_bitcast_fusion), channel_id=1, source_target_pairs={{0,24},{4,28},{8,16},{12,20},{16,8},{20,12},{24,0},{28,4},{1,25},{... | collective-permute-start | bytes 1572872 | tf_op jit(solution)/shard_map/ppermute | solution.py:28
  18.5 15.0 %collective-permute-start.1 = (bf16[256,512]{1,0:T(8,128)(2,1)}, bf16[256,512]{1,0:T(8,128)(2,1)S(1)}, u32[]{:S(2)}, u32[]{:S(2)}) collective-permute-start(bf16[256,512]{1,0:T(8,128)(2,1)} %get-tuple-element.33), channel_id=1, source_target_pairs={{0,1},{1,0},{2,3},{3,2},{4,5},{5,4},{6,7},{7,6},{8,9},{9,8},{10,11... | collective-permute-start | bytes 786440 | tf_op jit(solution)/shard_map/ppermute | solution.py:28
  18.5 15.0 %collective-permute-start.2 = (bf16[256,512]{1,0:T(8,128)(2,1)}, bf16[256,512]{1,0:T(8,128)(2,1)S(1)}, u32[]{:S(2)}, u32[]{:S(2)}) collective-permute-start(bf16[256,512]{1,0:T(8,128)(2,1)} %get-tuple-element.34), channel_id=1, source_target_pairs={{0,1},{1,0},{2,3},{3,2},{4,5},{5,4},{6,7},{7,6},{8,9},{9,8},{10,11... | collective-permute-start | bytes 786440 | tf_op jit(solution)/shard_map/ppermute | solution.py:28
  31.8 91.6 %collective-permute-start.16 = (bf16[1024,512]{1,0:T(8,128)(2,1)}, bf16[1024,512]{1,0:T(8,128)(2,1)}, u32[]{:S(2)}, u32[]{:S(2)}) collective-permute-start(bf16[1024,512]{1,0:T(8,128)(2,1)} %collective-permute-done.12.refs_8_), channel_id=1, source_target_pairs={{0,2},{1,3},{2,0},{3,1},{4,6},{5,7},{6,4},{7,5},{8,10},{9,11},{10,... | collective-permute-start | bytes 3145736 | tf_op jit(solution)/shard_map/ppermute | solution.py:28
  33.5 0.7 copy-start.7
  33.5 0.8 copy-start.8
  33.6 1.5 copy-start
  39.1 6.2 %copy-start.22 = (s32[256,2]{0,1:T(2,128)S(1)}, s32[256,2]{0,1:T(2,128)}, u32[]{:S(2)}) copy-start(s32[256,2]{0,1:T(2,128)} %param.20) | copy-start | bytes 6148
  39.1 30.2 %collective-permute-start.4 = (bf16[256,1024]{1,0:T(8,128)(2,1)}, bf16[256,1024]{1,0:T(8,128)(2,1)S(1)}, u32[]{:S(2)}, u32[]{:S(2)}) collective-permute-start(bf16[256,1024]{1,0:T(8,128)(2,1)} %get-tuple-element.36), channel_id=1, source_target_pairs={{0,2},{1,3},{2,0},{3,1},{4,6},{5,7},{6,4},{7,5},{8,10},{9,11},{10,... | collective-permute-start | bytes 1572872 | tf_op jit(solution)/shard_map/ppermute | solution.py:28
  43.7 36.9 %collective-permute-start.5 = (bf16[256,1024]{1,0:T(8,128)(2,1)}, bf16[256,1024]{1,0:T(8,128)(2,1)S(1)}, u32[]{:S(2)}, u32[]{:S(2)}) collective-permute-start(bf16[256,1024]{1,0:T(8,128)(2,1)} %get-tuple-element.39), channel_id=1, source_target_pairs={{0,2},{1,3},{2,0},{3,1},{4,6},{5,7},{6,4},{7,5},{8,10},{9,11},{10,... | collective-permute-start | bytes 1572872 | tf_op jit(solution)/shard_map/ppermute | solution.py:28
  45.4 78.8 %copy-start.10 = (bf16[512,512]{1,0:T(8,128)(2,1)}, bf16[512,512]{1,0:T(8,128)(2,1)S(1)}, u32[]{:S(2)}) copy-start(bf16[512,512]{1,0:T(8,128)(2,1)S(1)} %collective-permute-done.13.refs_9_) | copy-start | bytes 1572868
  45.4 78.0 %collective-permute-start.17 = (bf16[512,512]{1,0:T(8,128)(2,1)S(1)}, bf16[512,512]{1,0:T(8,128)(2,1)}, u32[]{:S(2)}, u32[]{:S(2)}) collective-permute-start(bf16[512,512]{1,0:T(8,128)(2,1)S(1)} %collective-permute-done.13.refs_9_), channel_id=1, source_target_pairs={{0,2},{1,3},{2,0},{3,1},{4,6},{5,7},{6,4},{7,5},{8,10},{9,11},{10,... | collective-permute-start | bytes 1572872 | tf_op jit(solution)/shard_map/ppermute | solution.py:28
  69.3 0.8 copy-start.12
  73.0 51.0 %collective-permute-start.6 = (bf16[192,1024]{1,0:T(8,128)(2,1)}, bf16[192,1024]{1,0:T(8,128)(2,1)S(1)}, u32[]{:S(2)}, u32[]{:S(2)}) collective-permute-start(bf16[192,1024]{1,0:T(8,128)(2,1)} %get-tuple-element.41), channel_id=1, source_target_pairs={{0,4},{4,0},{8,12},{12,8},{16,20},{20,16},{24,28},{28,24},{1,5},{5... | collective-permute-start | bytes 1179656 | tf_op jit(solution)/shard_map/ppermute | solution.py:28
  80.5 0.8 copy-start.11
  84.2 40.1 %collective-permute-start.7 = (bf16[192,1024]{1,0:T(8,128)(2,1)}, bf16[192,1024]{1,0:T(8,128)(2,1)S(1)}, u32[]{:S(2)}, u32[]{:S(2)}) collective-permute-start(bf16[192,1024]{1,0:T(8,128)(2,1)} %get-tuple-element.42), channel_id=1, source_target_pairs={{0,4},{4,0},{8,12},{12,8},{16,20},{20,16},{24,28},{28,24},{1,5},{5... | collective-permute-start | bytes 1179656 | tf_op jit(solution)/shard_map/ppermute | solution.py:28
  90.2 43.4 %collective-permute-start.8 = (bf16[192,1024]{1,0:T(8,128)(2,1)}, bf16[192,1024]{1,0:T(8,128)(2,1)S(1)}, u32[]{:S(2)}, u32[]{:S(2)}) collective-permute-start(bf16[192,1024]{1,0:T(8,128)(2,1)} %get-tuple-element.43), channel_id=1, source_target_pairs={{0,8},{4,12},{8,0},{12,4},{16,24},{20,28},{24,16},{28,20},{1,9},{5... | collective-permute-start | bytes 1179656 | tf_op jit(solution)/shard_map/ppermute | solution.py:28
  123.4 45.0 %collective-permute-start.14 = (bf16[1024,512]{1,0:T(8,128)(2,1)}, bf16[1024,512]{1,0:T(8,128)(2,1)S(1)}, u32[]{:S(2)}, u32[]{:S(2)}) collective-permute-start(bf16[1024,512]{1,0:T(8,128)(2,1)} %collective-permute-done.12.refs_8_), channel_id=1, source_target_pairs={{0,1},{1,0},{2,3},{3,2},{4,5},{5,4},{6,7},{7,6},{8,9},{9,8},{10,11... | collective-permute-start | bytes 3145736 | tf_op jit(solution)/shard_map/ppermute | solution.py:28
  123.4 45.0 %collective-permute-start.18 = (bf16[1024,512]{1,0:T(8,128)(2,1)}, bf16[1024,512]{1,0:T(8,128)(2,1)}, u32[]{:S(2)}, u32[]{:S(2)}) collective-permute-start(bf16[1024,512]{1,0:T(8,128)(2,1)} %collective-permute-done.16.refs_12_), channel_id=1, source_target_pairs={{0,1},{1,0},{2,3},{3,2},{4,5},{5,4},{6,7},{7,6},{8,9},{9,8},{10,11... | collective-permute-start | bytes 3145736 | tf_op jit(solution)/shard_map/ppermute | solution.py:28
  123.9 32.6 %copy-start.1 = (bf16[192,1024]{1,0:T(8,128)(2,1)}, bf16[192,1024]{1,0:T(8,128)(2,1)S(1)}, u32[]{:S(2)}) copy-start(bf16[192,1024]{1,0:T(8,128)(2,1)S(1)} %collective-permute-done.6.refs_2_) | copy-start | bytes 1179652
  123.9 18.1 %collective-permute-start.9 = (bf16[192,1024]{1,0:T(8,128)(2,1)}, bf16[192,1024]{1,0:T(8,128)(2,1)S(1)}, u32[]{:S(2)}, u32[]{:S(2)}) collective-permute-start(bf16[192,1024]{1,0:T(8,128)(2,1)} %get-tuple-element.44), channel_id=1, source_target_pairs={{0,8},{4,12},{8,0},{12,4},{16,24},{20,28},{24,16},{28,20},{1,9},{5... | collective-permute-start | bytes 1179656 | tf_op jit(solution)/shard_map/ppermute | solution.py:28
  124.2 32.3 %copy-start.2 = (bf16[192,1024]{1,0:T(8,128)(2,1)}, bf16[192,1024]{1,0:T(8,128)(2,1)S(1)}, u32[]{:S(2)}) copy-start(bf16[192,1024]{1,0:T(8,128)(2,1)S(1)} %collective-permute-done.7.refs_3_) | copy-start | bytes 1179652
  124.2 25.9 %collective-permute-start.10 = (bf16[192,1024]{1,0:T(8,128)(2,1)}, bf16[192,1024]{1,0:T(8,128)(2,1)S(1)}, u32[]{:S(2)}, u32[]{:S(2)}) collective-permute-start(bf16[192,1024]{1,0:T(8,128)(2,1)} %get-tuple-element.45), channel_id=1, source_target_pairs={{0,12},{4,8},{8,4},{12,0},{16,28},{20,24},{24,20},{28,16},{1,13},{... | collective-permute-start | bytes 1179656 | tf_op jit(solution)/shard_map/ppermute | solution.py:28
  133.6 22.9 %copy-start.3 = (bf16[192,1024]{1,0:T(8,128)(2,1)}, bf16[192,1024]{1,0:T(8,128)(2,1)S(1)}, u32[]{:S(2)}) copy-start(bf16[192,1024]{1,0:T(8,128)(2,1)S(1)} %collective-permute-done.8.refs_4_) | copy-start | bytes 1179652
  133.6 22.9 %collective-permute-start.11 = (bf16[192,1024]{1,0:T(8,128)(2,1)}, bf16[192,1024]{1,0:T(8,128)(2,1)S(1)}, u32[]{:S(2)}, u32[]{:S(2)}) collective-permute-start(bf16[192,1024]{1,0:T(8,128)(2,1)} %get-tuple-element.46), channel_id=1, source_target_pairs={{0,12},{4,8},{8,4},{12,0},{16,28},{20,24},{24,20},{28,16},{1,13},{... | collective-permute-start | bytes 1179656 | tf_op jit(solution)/shard_map/ppermute | solution.py:28
  142.0 14.5 %copy-start.4 = (bf16[192,1024]{1,0:T(8,128)(2,1)}, bf16[192,1024]{1,0:T(8,128)(2,1)S(1)}, u32[]{:S(2)}) copy-start(bf16[192,1024]{1,0:T(8,128)(2,1)S(1)} %collective-permute-done.9.refs_5_) | copy-start | bytes 1179652
  142.0 23.9 %collective-permute-start.15 = (bf16[512,512]{1,0:T(8,128)(2,1)}, bf16[512,512]{1,0:T(8,128)(2,1)}, u32[]{:S(2)}, u32[]{:S(2)}) collective-permute-start(bf16[512,512]{1,0:T(8,128)(2,1)} %copy-done.10), channel_id=1, source_target_pairs={{0,1},{1,0},{2,3},{3,2},{4,5},{5,4},{6,7},{7,6},{8,9},{9,8},{10,11... | collective-permute-start | bytes 1572872 | tf_op jit(solution)/shard_map/ppermute | solution.py:28
  150.1 6.4 %copy-start.5 = (bf16[192,1024]{1,0:T(8,128)(2,1)}, bf16[192,1024]{1,0:T(8,128)(2,1)S(1)}, u32[]{:S(2)}) copy-start(bf16[192,1024]{1,0:T(8,128)(2,1)S(1)} %collective-permute-done.10.refs_6_) | copy-start | bytes 1179652
  150.1 17.6 %collective-permute-start.19 = (bf16[512,512]{1,0:T(8,128)(2,1)}, bf16[512,512]{1,0:T(8,128)(2,1)}, u32[]{:S(2)}, u32[]{:S(2)}) collective-permute-start(bf16[512,512]{1,0:T(8,128)(2,1)} %collective-permute-done.17.refs_13_), channel_id=1, source_target_pairs={{0,1},{1,0},{2,3},{3,2},{4,5},{5,4},{6,7},{7,6},{8,9},{9,8},{10,11... | collective-permute-start | bytes 1572872 | tf_op jit(solution)/shard_map/ppermute | solution.py:28
  156.5 0.8 copy-start.6
  164.9 15.0 %collective-permute-start.23 = (bf16[96,2048]{1,0:T(8,128)(2,1)}, bf16[96,2048]{1,0:T(8,128)(2,1)S(1)}, u32[]{:S(2)}, u32[]{:S(2)}) collective-permute-start(bf16[96,2048]{1,0:T(8,128)(2,1)} %get-tuple-element.52), channel_id=1, source_target_pairs={{0,4},{4,0},{8,12},{12,8},{16,20},{20,16},{24,28},{28,24},{1,5},{5... | collective-permute-start | bytes 1179656 | tf_op jit(solution)/shard_map/ppermute | solution.py:28
  166.0 16.4 %collective-permute-start.24 = (bf16[96,2048]{1,0:T(8,128)(2,1)}, bf16[96,2048]{1,0:T(8,128)(2,1)S(1)}, u32[]{:S(2)}, u32[]{:S(2)}) collective-permute-start(bf16[96,2048]{1,0:T(8,128)(2,1)} %get-tuple-element.53), channel_id=1, source_target_pairs={{0,8},{4,12},{8,0},{12,4},{16,24},{20,28},{24,16},{28,20},{1,9},{5... | collective-permute-start | bytes 1179656 | tf_op jit(solution)/shard_map/ppermute | solution.py:28
  167.7 12.9 %copy-start.19 = (s32[256,2]{0,1:T(2,128)S(1)}, s32[256,2]{0,1:T(2,128)}, u32[]{:S(2)}) copy-start(s32[256,2]{0,1:T(2,128)} %select_reduce_fusion) | copy-start | bytes 6148
  167.7 13.7 %copy-start.21 = (f32[256,2]{0,1:T(2,128)S(1)}, f32[256,2]{0,1:T(2,128)}, u32[]{:S(2)}) copy-start(f32[256,2]{0,1:T(2,128)} %param.21) | copy-start | bytes 6148
  167.7 19.4 %collective-permute-start.25 = (bf16[96,2048]{1,0:T(8,128)(2,1)}, bf16[96,2048]{1,0:T(8,128)(2,1)S(1)}, u32[]{:S(2)}, u32[]{:S(2)}) collective-permute-start(bf16[96,2048]{1,0:T(8,128)(2,1)} %get-tuple-element.54), channel_id=1, source_target_pairs={{0,12},{4,8},{8,4},{12,0},{16,28},{20,24},{24,20},{28,16},{1,13},{... | collective-permute-start | bytes 1179656 | tf_op jit(solution)/shard_map/ppermute | solution.py:28
  168.4 1.0 copy-start.9
  177.1 18.3 %collective-permute-start.20 = (bf16[96,2048]{1,0:T(8,128)(2,1)}, bf16[96,2048]{1,0:T(8,128)(2,1)S(1)}, u32[]{:S(2)}, u32[]{:S(2)}) collective-permute-start(bf16[96,2048]{1,0:T(8,128)(2,1)} %get-tuple-element.48), channel_id=1, source_target_pairs={{0,4},{4,0},{8,12},{12,8},{16,20},{20,16},{24,28},{28,24},{1,5},{5... | collective-permute-start | bytes 1179656 | tf_op jit(solution)/shard_map/ppermute | solution.py:28
  178.2 17.3 %collective-permute-start.21 = (bf16[96,2048]{1,0:T(8,128)(2,1)}, bf16[96,2048]{1,0:T(8,128)(2,1)S(1)}, u32[]{:S(2)}, u32[]{:S(2)}) collective-permute-start(bf16[96,2048]{1,0:T(8,128)(2,1)} %get-tuple-element.49), channel_id=1, source_target_pairs={{0,8},{4,12},{8,0},{12,4},{16,24},{20,28},{24,16},{28,20},{1,9},{5... | collective-permute-start | bytes 1179656 | tf_op jit(solution)/shard_map/ppermute | solution.py:28
  179.9 7.2 %copy-start.13 = (bf16[96,2048]{1,0:T(8,128)(2,1)}, bf16[96,2048]{1,0:T(8,128)(2,1)S(1)}, u32[]{:S(2)}) copy-start(bf16[96,2048]{1,0:T(8,128)(2,1)S(1)} %collective-permute-done.23.refs_1_) | copy-start | bytes 1179652
  179.9 22.3 %collective-permute-start.22 = (bf16[96,2048]{1,0:T(8,128)(2,1)}, bf16[96,2048]{1,0:T(8,128)(2,1)S(1)}, u32[]{:S(2)}, u32[]{:S(2)}) collective-permute-start(bf16[96,2048]{1,0:T(8,128)(2,1)} %get-tuple-element.50), channel_id=1, source_target_pairs={{0,12},{4,8},{8,4},{12,0},{16,28},{20,24},{24,20},{28,16},{1,13},{... | collective-permute-start | bytes 1179656 | tf_op jit(solution)/shard_map/ppermute | solution.py:28
  182.4 4.7 %copy-start.14 = (bf16[96,2048]{1,0:T(8,128)(2,1)}, bf16[96,2048]{1,0:T(8,128)(2,1)S(1)}, u32[]{:S(2)}) copy-start(bf16[96,2048]{1,0:T(8,128)(2,1)S(1)} %collective-permute-done.24.refs_2_) | copy-start | bytes 1179652
  187.1 0.8 copy-start.15
  195.4 6.8 %copy-start.16 = (bf16[96,2048]{1,0:T(8,128)(2,1)}, bf16[96,2048]{1,0:T(8,128)(2,1)S(1)}, u32[]{:S(2)}) copy-start(bf16[96,2048]{1,0:T(8,128)(2,1)S(1)} %collective-permute-done.20.refs_1_) | copy-start | bytes 1179652
  195.4 6.8 %copy-start.17 = (bf16[96,2048]{1,0:T(8,128)(2,1)}, bf16[96,2048]{1,0:T(8,128)(2,1)S(1)}, u32[]{:S(2)}) copy-start(bf16[96,2048]{1,0:T(8,128)(2,1)S(1)} %collective-permute-done.21.refs_2_) | copy-start | bytes 1179652
  202.2 0.7 copy-start.18
  (1 other events, 0.6 us)
where the time goes:
time: 209 us; the launch traced here: 208 us
  waiting for transfers between devices  75.7 us (36%)
  starting transfers between devices  74.6 us (36%)
  Pallas kernels  42.7 us (20%)
  local copies, waits for them, and re-layouts  11.7 us (6%)
  other arithmetic  3.1 us (1%)
    ppermute x25, waiting for transfers between devices, crossed(): return lax.ppermute(value, axis, [(i, partner(i)) for i in range(peers)])  75.7 us
    ppermute x25, starting transfers between devices, crossed(): return lax.ppermute(value, axis, [(i, partner(i)) for i in range(peers)])  71.2 us
    pallas_call x2, Pallas kernels, expert(): pl.pallas_call(functools.partial(expert_kernel, group, chunks, swapped, p...  15.2 us
    pallas_call x2, Pallas kernels, combined(): pl.pallas_call(functools.partial(combine_kernel, group, side), grid=(step...  9.86 us
    pallas_call x2, Pallas kernels, projections(): pl.pallas_call(functools.partial(project_kernel, count), grid=(steps,), i...  8.27 us
    unnamed x47, local copies, waits for them, and re-layouts  7.05 us
    pallas_call x2, Pallas kernels, rows_to_send(): pl.pallas_call(functools.partial(send_kernel, len(parts)), in_specs=[VMEM...  5.71 us
  transfers between devices with their start and end apart: 26, of which 10 were waited for; matrix products, arithmetic and copies ran while one was open for 4% of the time, Pallas kernels for 15%

commit v1 on v0

v1 whole, which is shorter than its diff:
```python
import functools

import jax
import jax.numpy as jnp
from jax import lax
from jax.experimental import pallas as pl
from jax.experimental.pallas import tpu as pltpu
from jax.sharding import PartitionSpec as P


HALO = 16
CHUNKS = 2

f32 = jnp.float32
bf16 = jnp.bfloat16

VMEM = pl.BlockSpec(memory_space=pltpu.VMEM)
SMEM = pl.BlockSpec(memory_space=pltpu.SMEM)
ANY = pl.BlockSpec(memory_space=pl.ANY)


def dot(a, b):
    return jnp.dot(a, b, preferred_element_type=f32)


def flipped(value, axis, bits):
    return lax.ppermute(value, axis, [(i, i ^ bits) for i in range(lax.axis_size(axis))])


def reversed_pairs(count):
    return lambda i: (count - 2 - (i // 2) * 2) + i % 2


def cut_kernel(x_ref, gate_ref, up_ref, down_ref, tail_ref, *rest):
    gate_out, up_out, down_out, sems = rest
    part = down_out.shape[1]
    span = pl.ds(pl.multiple_of(lax.axis_index("tp") * part, part), part)
    rows = x_ref.shape[0]
    moves = [
        pltpu.make_async_copy(source, target, sems.at[n])
        for n, (source, target) in enumerate(
            [
                (x_ref.at[rows - HALO : rows, :], tail_ref),
                (gate_ref.at[0, span, :], gate_out),
                (up_ref.at[0, span, :], up_out),
                (down_ref.at[0, :, span], down_out),
            ]
        )
    ]
    for move in moves:
        move.start()
    for move in moves:
        move.wait()


def cut_out(pooled_in, gate_weight, up_weight, down_weight):
    part = gate_weight.shape[1] // lax.axis_size("tp")
    hidden_units = gate_weight.shape[2]
    return pl.pallas_call(
        cut_kernel,
        in_specs=[ANY] * 4,
        out_specs=[VMEM] * 4,
        out_shape=[
            jax.ShapeDtypeStruct((HALO, pooled_in.shape[1]), bf16),
            jax.ShapeDtypeStruct((part, hidden_units), bf16),
            jax.ShapeDtypeStruct((part, hidden_units), bf16),
            jax.ShapeDtypeStruct((hidden_units, part), bf16),
        ],
        scratch_shapes=[pltpu.SemaphoreType.DMA((4,))],
        name="cut",
    )(pooled_in, gate_weight, up_weight, down_weight)


def pool_kernel(halo_ref, x_ref, map_ref, scale_ref, *rest):
    *kept_refs, given_ref = rest
    blocks = 2 * len(kept_refs)
    rows = x_ref.shape[0] // blocks
    tp_at = lax.axis_index("tp")
    first = lax.axis_index("sp") * x_ref.shape[0]
    window = jnp.left_shift(jnp.int32(2), tp_at)
    behind = lax.broadcasted_iota(jnp.int32, (rows, rows), 0) - lax.broadcasted_iota(
        jnp.int32, (rows, rows), 1
    )
    band = jnp.where((behind >= 0) & (behind < window), 1.0, 0.0).astype(bf16)
    early = (
        HALO
        + lax.broadcasted_iota(jnp.int32, (HALO, HALO), 0)
        - lax.broadcasted_iota(jnp.int32, (HALO, HALO), 1)
    )
    early_band = jnp.where(early < window, 1.0, 0.0).astype(bf16)
    for k in [*range(1, blocks, 2), *range(0, blocks, 2)]:
        block = tp_at ^ k
        x = x_ref[pl.ds(pl.multiple_of(block * rows, rows), rows), :]
        before = pl.multiple_of(jnp.maximum(block * rows - HALO, 0), HALO)
        tail = jnp.where(block == 0, halo_ref[...], x_ref[pl.ds(before, HALO), :])
        sums = dot(band, x)
        sums = jnp.concatenate([sums[:HALO] + dot(early_band, tail), sums[HALO:]], axis=0)
        position = first + block * rows + lax.broadcasted_iota(jnp.int32, (rows, 1), 0)
        share = 1.0 / jnp.minimum(position + 1, window).astype(f32)
        contrast = (sums * share - x.astype(f32)).astype(bf16)
        pooled = (dot(contrast, map_ref[0]) * scale_ref[...]).astype(bf16)
        if k % 2:
            given_ref[k // 2 * rows : (k // 2 + 1) * rows, :] = pooled
        else:
            kept_refs[k // 2][...] = pooled


def pooled_blocks(tail, pooled_in, group_map, pool_scale):
    rows, width = pooled_in.shape
    replicas = lax.axis_size("tp")
    peers = lax.axis_size("sp")
    halo = lax.ppermute(tail, "sp", [(i, i + 1) for i in range(peers - 1)])
    return pl.pallas_call(
        pool_kernel,
        in_specs=[VMEM] * 4,
        out_specs=[VMEM] * (replicas // 2 + 1),
        out_shape=[jax.ShapeDtypeStruct((rows // replicas, width), bf16)] * (replicas // 2)
        + [jax.ShapeDtypeStruct((rows // 2, width), bf16)],
        name="pool",
        compiler_params=pltpu.CompilerParams(vmem_limit_bytes=12 << 20),
    )(halo, pooled_in, group_map, pool_scale[None, :])


def project_kernel(count, *refs):
    mine = refs[:count]
    mates = refs[count : 2 * count]
    w_mine, w_mate = refs[2 * count : 2 * count + 2]
    outs = refs[-count - 1 : -1]
    residual = refs[2 * count + 2 : -count - 1]
    lines = refs[-1]
    rows, width = mine[0].shape

    @pl.when(pl.program_id(0) == 0)
    def _():
        for n in range(count):
            lines[n * rows : (n + 1) * rows, :width] = mine[n][...]
            lines[n * rows : (n + 1) * rows, width:] = mates[n][...]

    sums = dot(lines[:, :width], w_mine[...]) + dot(lines[:, width:], w_mate[...])
    for n in range(count):
        part = sums[n * rows : (n + 1) * rows]
        if residual:
            part = part + residual[0][...].astype(f32)
        outs[n][...] = part.astype(outs[n].dtype)


def projections(mine, mates, first, w_mine, w_mate, residual, chunk, columns):
    count = len(mine)
    rows, width = mine[0].shape
    step = min(512, columns)
    steps = columns // step
    whole = pl.BlockSpec((rows, width), lambda j: (0, 0))
    weight = pl.BlockSpec((width, step), lambda j: (0, chunk * steps + j))
    tile = pl.BlockSpec((rows, step), lambda j: (0, j))
    dtype = f32 if residual else bf16
    return pl.pallas_call(
        functools.partial(project_kernel, count),
        grid=(steps,),
        in_specs=[whole] * count
        + [pl.BlockSpec((rows, width), lambda j, n=n: (first + n, 0)) for n in range(count)]
        + [weight, weight]
        + [pl.BlockSpec((rows, step), lambda j: (0, chunk * steps + j))] * len(residual),
        out_specs=[tile] * count,
        out_shape=[jax.ShapeDtypeStruct((rows, columns), dtype)] * count,
        scratch_shapes=[pltpu.VMEM((count * rows, 2 * width), bf16)],
        name="project",
        compiler_params=pltpu.CompilerParams(vmem_limit_bytes=16 << 20),
    )(*mine, *([mates] * count), w_mine, w_mate, *residual)


def send_kernel(others, slots_ref, own_ref, *refs):
    parts = refs[:others]
    middle_ref, *outs = refs[others:]
    total = own_ref[...]
    for part in parts:
        total = total + part[...].astype(f32)
    middle = total.astype(bf16)
    middle_ref[...] = middle
    length = outs[0].shape[0]
    rows = own_ref.shape[0]
    for k, out in enumerate(outs):
        slot = k * length + lax.broadcasted_iota(jnp.int32, (length, rows), 0)
        hit = slot == slots_ref[0:1, :]
        for j in range(1, slots_ref.shape[0]):
            hit = hit | (slot == slots_ref[j : j + 1, :])
        out[...] = dot(jnp.where(hit, 1.0, 0.0).astype(bf16), middle).astype(bf16)


def rows_to_send(slots_t, own, parts, group, length):
    rows, columns = own.shape
    return pl.pallas_call(
        functools.partial(send_kernel, len(parts)),
        in_specs=[VMEM] * (2 + len(parts)),
        out_specs=[VMEM] * (1 + group),
        out_shape=[jax.ShapeDtypeStruct((rows, columns), bf16)]
        + [jax.ShapeDtypeStruct((length, columns), bf16)] * group,
        name="send",
        compiler_params=pltpu.CompilerParams(vmem_limit_bytes=12 << 20),
    )(slots_t, own, *parts)


def expert_kernel(group, chunks, side, pieces, gain_ref, *refs):
    row_refs = refs[: group * chunks]
    weights = refs[group * chunks : -group - 1]
    outs = refs[-group - 1 : -1]
    lines = refs[-1]
    capacity = outs[0].shape[0]
    part = lines.shape[1] // pieces
    hidden_units = weights[0].shape[-1]
    swapped = len(weights) > 3
    tp_at = lax.axis_index("tp")
    mine = slice(side * capacity, (side + 1) * capacity)
    for p in range(group):
        blocks = [
            (ref[mine, :] if ref.shape[0] > capacity else ref[...]).astype(f32)
            for ref in row_refs[p * chunks : (p + 1) * chunks]
        ]
        square = sum(jnp.sum(b * b, axis=1, keepdims=True) for b in blocks)
        factor = lax.rsqrt(square / lines.shape[1] + 1e-06)
        at = 0
        for b in blocks:
            span = slice(at, at + b.shape[1])
            lines[p * capacity : (p + 1) * capacity, span] = (
                b * factor * gain_ref[:, span]
            ).astype(bf16)
            at += b.shape[1]

    def piece(k):
        if swapped:
            span = pl.ds(pl.multiple_of((tp_at ^ k) * part, part), part)
            gate, up, down = (ref[...] for ref in weights[3 * k : 3 * k + 3])
        else:
            span = slice(k * part, (k + 1) * part)
            gate, up, down = weights[0][0, span, :], weights[1][0, span, :], weights[2][0, :, span]
        return span, gate, up, down

    gate_part = jnp.zeros((group * capacity, hidden_units), f32)
    up_part = jnp.zeros((group * capacity, hidden_units), f32)
    for k in range(pieces):
        span, gate, up, _ = piece(k)
        x = lines[:, span]
        gate_part = gate_part + dot(x, gate)
        up_part = up_part + dot(x, up)
    hidden = (gate_part / (1.0 + jnp.exp(-gate_part)) * up_part).astype(bf16)
    for k in range(pieces):
        span, _, _, down = piece(k)
        made = dot(hidden, down).astype(bf16)
        for p in range(group):
            outs[p][:, span] = made[p * capacity : (p + 1) * capacity]


def expert(row_blocks, side, capacity, norm_gain, weights):
    group = len(row_blocks)
    chunks = len(row_blocks[0])
    width = norm_gain.shape[0]
    flat = [b for blocks in row_blocks for b in blocks]
    return pl.pallas_call(
        functools.partial(expert_kernel, group, chunks, side, lax.axis_size("tp")),
        in_specs=[VMEM] * (1 + len(flat) + len(weights)),
        out_specs=[VMEM] * group,
        out_shape=[jax.ShapeDtypeStruct((capacity, width), bf16)] * group,
        scratch_shapes=[pltpu.VMEM((group * capacity, width), bf16)],
        name="expert_far" if side else "expert_own",
        compiler_params=pltpu.CompilerParams(vmem_limit_bytes=28 << 20),
    )(norm_gain[None, :], *flat, *weights)


def combine_kernel(group, side, slots_ref, share_ref, *refs):
    row_refs = refs[:group]
    base_refs = refs[group:-2]
    out_ref, back = refs[-2:]
    capacity = row_refs[0].shape[0]
    rows = out_ref.shape[0]
    for p in range(group):
        back[p * capacity : (p + 1) * capacity, :] = row_refs[p][...]
    column = lax.broadcasted_iota(jnp.int32, (rows, group * capacity), 1)
    peer = sum((column >= p * capacity).astype(jnp.int32) for p in range(1, group))
    slot = column + (peer + side) * capacity
    weigh = jnp.zeros((rows, group * capacity), f32)
    for j in range(slots_ref.shape[1]):
        weigh = weigh + jnp.where(slot == slots_ref[:, j : j + 1], share_ref[:, j : j + 1], 0.0)
    high = weigh.astype(bf16)
    low = (weigh - high.astype(f32)).astype(bf16)
    at = 0
    for base in base_refs:
        span = slice(at, at + base.shape[1])
        total = base[...].astype(f32) + dot(high, back[:, span]) + dot(low, back[:, span])
        out_ref[:, span] = total.astype(out_ref.dtype)
        at += base.shape[1]


def combined(slots, shares, bases, returned, side, dtype):
    group = len(returned)
    capacity, width = returned[0].shape
    steps = 1
    tile = lambda v: pl.BlockSpec((v.shape[0], v.shape[1] // steps), lambda j: (0, j))
    small = pl.BlockSpec(slots.shape, lambda j: (0, 0))
    out = jax.ShapeDtypeStruct((slots.shape[0], width), dtype)
    return pl.pallas_call(
        functools.partial(combine_kernel, group, side),
        grid=(steps,),
        in_specs=[small, small] + [tile(v) for v in [*returned, *bases]],
        out_specs=tile(out),
        out_shape=out,
        scratch_shapes=[pltpu.VMEM((group * capacity, width // steps), bf16)],
        name="combine",
        compiler_params=pltpu.CompilerParams(vmem_limit_bytes=16 << 20),
    )(slots, shares, *returned, *bases)


def body(
    pooled_in,
    group_map,
    pool_scale,
    out_weight,
    residual,
    norm_gain,
    gate_weight,
    up_weight,
    down_weight,
    route_expert,
    route_score,
):
    experts = lax.axis_size("sp")
    replicas = lax.axis_size("tp")
    sp_at = lax.axis_index("sp")
    rows, width = residual.shape
    top = route_expert.shape[1]
    capacity = max(2, 3 * rows * top // (2 * experts))
    capacity = -(-capacity // 16) * 16
    group = experts // 2
    other_half = reversed_pairs(experts)
    columns = width // CHUNKS

    mate_weight = flipped(out_weight, "tp", 1)
    tail, *pieces = cut_out(pooled_in, gate_weight, up_weight, down_weight)
    pairs = [(i, other_half(i)) for i in range(experts)]
    copied = {0: [lax.ppermute(v, "sp", pairs) for v in pieces]}

    here = jnp.arange(experts, dtype=jnp.int32)
    owner = jnp.where(here // group == sp_at // group, here, other_half(here))
    block_of = 2 * (owner ^ sp_at) + (owner != here).astype(jnp.int32)
    named = route_expert[:, :, None] == here[None, None, :]
    hits = jnp.any(named, axis=1)
    earlier = jnp.arange(rows)[:, None] > jnp.arange(rows)[None, :]
    rank = dot(earlier.astype(bf16), hits.astype(bf16)).astype(jnp.int32)
    slot_of = block_of[None, :] * capacity + rank
    slots = jnp.sum(jnp.where(named, slot_of[:, None, :], 0), axis=2)
    slots_t = slots.T
    shares = route_score / jnp.sum(route_score, axis=1, keepdims=True)

    pooled = pooled_blocks(tail, pooled_in, group_map, pool_scale)
    *mine, given = pooled
    mates = flipped(given, "tp", 1)
    parts = []
    for c in range(CHUNKS):
        leaving = projections(
            mine[1:], mates, 1, out_weight, mate_weight, [], c, columns
        )
        parts.append([flipped(v, "tp", 2 * n + 2) for n, v in enumerate(leaving)])
    middles = []
    arrived = [[[] for _ in range(group)] for _ in range(2)]
    for c in range(CHUNKS):
        (own,) = projections(mine[:1], mates, 0, out_weight, mate_weight, [residual], c, columns)
        split = 2 if c == CHUNKS - 1 else 1
        middle, *outgoing = rows_to_send(
            slots_t, own, parts[c], split * group, 2 * capacity // split
        )
        middles.append(middle)
        for k in range(group):
            rows_of = [
                v if k == 0 else flipped(v, "sp", k)
                for v in outgoing[split * k : split * (k + 1)]
            ]
            for side in range(2):
                arrived[side][k].append(rows_of[side % split])

    bit = replicas // 2
    while bit:
        for k, held in list(copied.items()):
            copied[k ^ bit] = [flipped(v, "tp", bit) for v in held]
        bit //= 2
    copied = [v for k in range(replicas) for v in copied[k]]

    def sent_back(made):
        return [made[0]] + [flipped(made[k], "sp", k) for k in range(1, group)]

    made = expert(arrived[0], 0, capacity, norm_gain, (gate_weight, up_weight, down_weight))
    back = sent_back(made)
    made = expert(arrived[1], 1, capacity, norm_gain, copied)
    far_back = sent_back(made)
    total = combined(slots, shares, middles, back, 0, f32)
    return combined(slots, shares, [total], far_back, 1, bf16)


def solution(mesh):
    in_specs = (
        P("sp", "tp"),
        P("tp", None, None),
        P("tp"),
        P("tp", None),
        P(("sp", "tp"), None),
        P(),
        P("sp", None, None),
        P("sp", None, None),
        P("sp", None, None),
        P(("sp", "tp"), None),
        P(("sp", "tp"), None),
    )
    out_specs = P(("sp", "tp"), None)
    return jax.shard_map(body, mesh=mesh, in_specs=in_specs, out_specs=out_specs, check_vma=False)
```

time: 209 us -> 184 us (0.88)
  Pallas kernels: 42.7 us -> 30.5 us
  local copies, waits for them, and re-layouts: 11.7 us -> 3.08 us
  other arithmetic: 3.1 us -> 0.2 us
    pallas_call x3 -> x4, Pallas kernels: 18.9 us -> 13.7 us  [the longest x2 9.43 us: expert(): pl.pallas_call(functools.partial(expert_kernel, group, chunks, side, lax....]
    pallas_call x2, Pallas kernels: 9.86 us -> 4.99 us  [combined(): pl.pallas_call(functools.partial(combine_kernel, group, side), grid=(step...]
    unnamed x47 -> x31, local copies, waits for them, and re-layouts: 7.05 us -> 2.95 us
    dynamic_slice x2 -> x0, local copies, waits for them, and re-layouts: 3.17 us -> none  [the longest x1 1.9 us: body(): down = lax.dynamic_slice_in_dim(down_weight[0], start, part, 1)]
    pallas_call x2, Pallas kernels: 5.71 us -> 2.65 us  [rows_to_send(): pl.pallas_call(functools.partial(send_kernel, len(parts)), in_specs=[VMEM...]
    ppermute x26 -> x32, starting transfers between devices: 74.6 us -> 72.8 us  [the longest x28 59.2 us: flipped(): lax.ppermute(value, axis, [(i, i ^ bits) for i in range(lax.axis_size(axi...]
    ppermute x26 -> x32, waiting for transfers between devices: 75.7 us -> 76.9 us  [the longest x28 54 us: flipped(): lax.ppermute(value, axis, [(i, i ^ bits) for i in range(lax.axis_size(axi...]
    pallas_call x2 -> x4, Pallas kernels: 8.27 us -> 9.19 us  [projections(): pl.pallas_call(functools.partial(project_kernel, count), grid=(steps,), i...]
  transfers between devices with their start and end apart: 26 -> 32, of which waited for: 10 -> 12; matrix products, arithmetic and copies ran while one was open for 4% -> 0% of each run, Pallas kernels for 15% -> 14%
where the time goes in v1:
time: 184 us
  waiting for transfers between devices  76.9 us (42%)
  starting transfers between devices  72.8 us (40%)
  Pallas kernels  30.5 us (17%)
  local copies, waits for them, and re-layouts  3.08 us (2%)
    ppermute x28, starting transfers between devices, flipped(): lax.ppermute(value, axis, [(i, i ^ bits) for i in range(lax.axis_size(axi...  59.2 us
    ppermute x28, waiting for transfers between devices, flipped(): lax.ppermute(value, axis, [(i, i ^ bits) for i in range(lax.axis_size(axi...  54 us
    ppermute x3, waiting for transfers between devices, body(): copied = {0: [lax.ppermute(v, 'sp', pairs) for v in pieces]}  21.3 us
    pallas_call x2, Pallas kernels, expert(): pl.pallas_call(functools.partial(expert_kernel, group, chunks, side, lax....  9.43 us
    pallas_call x4, Pallas kernels, projections(): pl.pallas_call(functools.partial(project_kernel, count), grid=(steps,), i...  9.19 us
    ppermute x3, starting transfers between devices, body(): copied = {0: [lax.ppermute(v, 'sp', pairs) for v in pieces]}  9.16 us
    pallas_call x2, Pallas kernels, combined(): pl.pallas_call(functools.partial(combine_kernel, group, side), grid=(step...  4.99 us
    ppermute x1, starting transfers between devices, pooled_blocks(): halo = lax.ppermute(tail, 'sp', [(i, i + 1) for i in range(peers - 1)])  4.43 us
  transfers between devices with their start and end apart: 32, of which 12 were waited for; matrix products, arithmetic and copies ran while one was open for 0% of the time, Pallas kernels for 14%

profile of v1, /device:TPU:0, one launch (start us, length us, event | category | flops | bytes accessed | tf_op | source)
XLA Modules:
  0.0 184.0 jit_solution(11621027292329517864)
XLA Ops:
  0.0 0.5 collective-permute-start.2
  0.5 2.7 %cut.1 = (bf16[16,512]{1,0:T(8,128)(2,1)}, bf16[512,512]{1,0:T(8,128)(2,1)}, bf16[512,512]{1,0:T(8,128)(2,1)}, bf16[512,512]{1,0:T(8,128)(2,1)}) custom-call(bf16[1024,512]{1,0:T(8,128)(2,1)} %x_ref.3, bf16[1,2048,512]{2,1,0:T(8,128)(2,1)} %refs_8_.1, bf16[1,2048,512]{2,1,0:T(8,128)(2,1)} %refs_9_.1, bf16[1,512,2048]{2,1,0:T(8,128)(2,1)} %refs_10_.1), custom_call_target="tpu_custom_call" | custom-call | tf_op jit(solution)/shard_map/cut/pallas_call | solution.py:59
  3.2 4.4 %collective-permute-start = (bf16[16,512]{1,0:T(8,128)(2,1)}, bf16[16,512]{1,0:T(8,128)(2,1)S(1)}, u32[]{:S(2)}, u32[]{:S(2)}) collective-permute-start(bf16[16,512]{1,0:T(8,128)(2,1)} %get-tuple-element.34), channel_id=1, source_target_pairs={{0,4},{4,8},{8,12},{12,16},{16,20},{20,24},{24,28},{1,5},{5,9},{9,... | collective-permute-start | bytes 49160 | tf_op jit(solution)/shard_map/ppermute | solution.py:112
  7.6 1.6 collective-permute-done.halo_ref
  9.3 1.0 copy-done.8
  10.3 1.5 pool.1
  12.0 5.3 %collective-permute-start.11 = (bf16[512,512]{1,0:T(8,128)(2,1)}, bf16[512,512]{1,0:T(8,128)(2,1)S(1)}, u32[]{:S(2)}, u32[]{:S(2)}) collective-permute-start(bf16[512,512]{1,0:T(8,128)(2,1)} %get-tuple-element.46), channel_id=1, source_target_pairs={{0,24},{4,28},{8,16},{12,20},{16,8},{20,12},{24,0},{28,4},{1,25},{... | collective-permute-start | bytes 1572872 | tf_op jit(solution)/shard_map/ppermute | solution.py:338
  17.4 3.7 %collective-permute-start.13 = (bf16[512,512]{1,0:T(8,128)(2,1)}, bf16[512,512]{1,0:T(8,128)(2,1)}, u32[]{:S(2)}, u32[]{:S(2)}) collective-permute-start(bf16[512,512]{1,0:T(8,128)(2,1)} %get-tuple-element.48), channel_id=1, source_target_pairs={{0,24},{4,28},{8,16},{12,20},{16,8},{20,12},{24,0},{28,4},{1,25},{... | collective-permute-start | bytes 1572872 | tf_op jit(solution)/shard_map/ppermute | solution.py:338
  21.1 2.8 %project.7 = bf16[256,1024]{1,0:T(8,128)(2,1)} custom-call(bf16[256,512]{1,0:T(8,128)(2,1)S(1)} %get-tuple-element.37.refs_0_, bf16[512,512]{1,0:T(8,128)(2,1)S(1)} %collective-permute-done.1.refs_1_, bf16[512,2048]{1,0:T(8,128)(2,1)S(1)} %copy-done, bf16[512,2048]{1,0:T(8,128)(2,1)} %collective-permute-done.2.refs_3_), custom_call_target="tpu_custom_call" | custom-call | tf_op jit(solution)/shard_map/project/pallas_call | solution.py:156
  23.9 1.5 collective-permute-start.4
  25.4 5.0 %collective-permute-done.11.refs_8_ = bf16[512,512]{1,0:T(8,128)(2,1)S(1)} collective-permute-done((bf16[512,512]{1,0:T(8,128)(2,1)}, bf16[512,512]{1,0:T(8,128)(2,1)S(1)}, u32[]{:S(2)}, u32[]{:S(2)}) %collective-permute-start.11) | collective-permute-done | bytes 524320 | tf_op jit(solution)/shard_map/ppermute | solution.py:338
  30.4 1.5 collective-permute-start.17
  31.9 9.8 %collective-permute-done.12.refs_9_ = bf16[512,512]{1,0:T(8,128)(2,1)} collective-permute-done((bf16[512,512]{1,0:T(8,128)(2,1)}, bf16[512,512]{1,0:T(8,128)(2,1)}, u32[]{:S(2)}, u32[]{:S(2)}) %collective-permute-start.12) | collective-permute-done | bytes 524320 | tf_op jit(solution)/shard_map/ppermute | solution.py:338
  41.7 1.5 collective-permute-start.18
  43.2 0.9 copy-done.7
  44.2 2.0 %project.5 = bf16[256,1024]{1,0:T(8,128)(2,1)S(1)} custom-call(bf16[256,512]{1,0:T(8,128)(2,1)S(1)} %copy-done.7, bf16[512,512]{1,0:T(8,128)(2,1)S(1)} %collective-permute-done.1.refs_1_, bf16[512,2048]{1,0:T(8,128)(2,1)S(1)} %copy-done, bf16[512,2048]{1,0:T(8,128)(2,1)} %collective-permute-done.2.refs_3_), custom_call_target="tpu_custom_call" | custom-call | tf_op jit(solution)/shard_map/project/pallas_call | solution.py:156
  46.2 6.5 %collective-permute-done.13.refs_10_ = bf16[512,512]{1,0:T(8,128)(2,1)} collective-permute-done((bf16[512,512]{1,0:T(8,128)(2,1)}, bf16[512,512]{1,0:T(8,128)(2,1)}, u32[]{:S(2)}, u32[]{:S(2)}) %collective-permute-start.13) | collective-permute-done | bytes 524320 | tf_op jit(solution)/shard_map/ppermute | solution.py:338
  52.7 1.5 collective-permute-start.3
  54.2 0.6 collective-permute-start.19
  55.1 2.1 %project.4.own_ref = f32[256,1024]{1,0:T(8,128)S(1)} custom-call(bf16[256,512]{1,0:T(8,128)(2,1)S(1)} %get-tuple-element.35.refs_0_, bf16[512,512]{1,0:T(8,128)(2,1)S(1)} %collective-permute-done.1.refs_1_, bf16[512,2048]{1,0:T(8,128)(2,1)S(1)} %copy-done, bf16[512,2048]{1,0:T(8,128)(2,1)} %collective-permute-done.2.refs_3_, bf16[256,2048]{1,0:T(8,128)(2,1)S(1)} %copy-done.4), custom_call_target="tpu_custom_call" | custom-call | tf_op jit(solution)/shard_map/project/pallas_call | solution.py:156
  57.2 2.3 %project.6.own_ref = f32[256,1024]{1,0:T(8,128)S(1)} custom-call(bf16[256,512]{1,0:T(8,128)(2,1)S(1)} %get-tuple-element.35.refs_0_, bf16[512,512]{1,0:T(8,128)(2,1)S(1)} %collective-permute-done.1.refs_1_, bf16[512,2048]{1,0:T(8,128)(2,1)S(1)} %copy-done, bf16[512,2048]{1,0:T(8,128)(2,1)} %collective-permute-done.2.refs_3_, bf16[256,2048]{1,0:T(8,128)(2,1)S(1)} %copy-done.4), custom_call_target="tpu_custom_call" | custom-call | tf_op jit(solution)/shard_map/project/pallas_call | solution.py:156
  59.5 2.0 %send.3 = (bf16[256,1024]{1,0:T(8,128)(2,1)S(1)}, bf16[96,1024]{1,0:T(8,128)(2,1)S(1)}, bf16[96,1024]{1,0:T(8,128)(2,1)S(1)}, bf16[96,1024]{1,0:T(8,128)(2,1)S(1...) custom-call(s32[2,256]{1,0:T(2,128)S(1)} %bitcast.6, ...), custom_call_target="tpu_custom_call" | custom-call | tf_op jit(solution)/shard_map/send/pallas_call | solution.py:191
  61.5 11.1 %collective-permute-done.3.refs_0_ = bf16[256,1024]{1,0:T(8,128)(2,1)S(1)} collective-permute-done((bf16[256,1024]{1,0:T(8,128)(2,1)S(1)}, bf16[256,1024]{1,0:T(8,128)(2,1)S(1)}, u32[]{:S(2)}, u32[]{:S(2)}) %collective-permute-start.3) | collective-permute-done | bytes 524320 | tf_op jit(solution)/shard_map/ppermute | solution.py:27
  72.7 0.6 collective-permute-start.26
  73.3 0.6 send.2
  73.9 1.5 collective-permute-start.5
  75.4 28.9 %collective-permute-start.7 = (bf16[192,1024]{1,0:T(8,128)(2,1)S(1)}, bf16[192,1024]{1,0:T(8,128)(2,1)S(1)}, u32[]{:S(2)}, u32[]{:S(2)}) collective-permute-start(bf16[192,1024]{1,0:T(8,128)(2,1)S(1)} %get-tuple-element.42), channel_id=1, source_target_pairs={{0,8},{4,12},{8,0},{12,4},{16,24},{20,28},{24,16},{28,20},{1,9},{5... | collective-permute-start | bytes 1179656 | tf_op jit(solution)/shard_map/ppermute | solution.py:27
  104.4 7.7 %collective-permute-start.28 = (bf16[96,1024]{1,0:T(8,128)(2,1)S(1)}, bf16[96,1024]{1,0:T(8,128)(2,1)S(1)}, u32[]{:S(2)}, u32[]{:S(2)}) collective-permute-start(bf16[96,1024]{1,0:T(8,128)(2,1)S(1)} %get-tuple-element.56), channel_id=1, source_target_pairs={{0,12},{4,8},{8,4},{12,0},{16,28},{20,24},{24,20},{28,16},{1,13},{... | collective-permute-start | bytes 589832 | tf_op jit(solution)/shard_map/ppermute | solution.py:27
  112.1 6.4 %collective-permute-done.27.refs_5_ = bf16[96,1024]{1,0:T(8,128)(2,1)S(1)} collective-permute-done((bf16[96,1024]{1,0:T(8,128)(2,1)S(1)}, bf16[96,1024]{1,0:T(8,128)(2,1)S(1)}, u32[]{:S(2)}, u32[]{:S(2)}) %collective-permute-start.27) | collective-permute-done | bytes 196640 | tf_op jit(solution)/shard_map/ppermute | solution.py:27
  118.5 4.3 %collective-permute-done.28.refs_7_ = bf16[96,1024]{1,0:T(8,128)(2,1)S(1)} collective-permute-done((bf16[96,1024]{1,0:T(8,128)(2,1)S(1)}, bf16[96,1024]{1,0:T(8,128)(2,1)S(1)}, u32[]{:S(2)}, u32[]{:S(2)}) %collective-permute-start.28) | collective-permute-done | bytes 196640 | tf_op jit(solution)/shard_map/ppermute | solution.py:27
  122.8 0.5 collective-permute-start.20
  123.4 5.1 %collective-permute-done.9.refs_6_ = bf16[192,1024]{1,0:T(8,128)(2,1)S(1)} collective-permute-done((bf16[192,1024]{1,0:T(8,128)(2,1)S(1)}, bf16[192,1024]{1,0:T(8,128)(2,1)S(1)}, u32[]{:S(2)}, u32[]{:S(2)}) %collective-permute-start.9) | collective-permute-done | bytes 393248 | tf_op jit(solution)/shard_map/ppermute | solution.py:27
  128.5 3.8 %expert_own.1 = (bf16[96,2048]{1,0:T(8,128)(2,1)S(1)}, bf16[96,2048]{1,0:T(8,128)(2,1)S(1)}, bf16[96,2048]{1,0:T(8,128)(2,1)}, bf16[96,2048]{1,0:T(8,128)(2,1)}) custom-call(f32[1,2048]{1,0:T(1,128)S(1)} %bitcast.4, bf16[192,1024]{1,0:T(8,128)(2,1)S(1)} %get-tuple-element.38.refs_0_, bf16[96,1024]{1,0:T(8,128)(2,1)S(1)} %get-tuple-element.53.refs_1_, ...), custom_call_target="tpu_custom_call" | custom-call | tf_op jit(solution)/shard_map/expert_own/pallas_call | solution.py:257
  132.4 1.4 collective-permute-start.29
  133.8 0.6 collective-permute-start.6
  134.4 1.7 collective-permute-start.8
  136.1 1.1 collective-permute-start.10
  137.3 1.7 collective-permute-start.30
  139.0 13.3 %collective-permute-done.6.refs_3_ = bf16[96,1024]{1,0:T(8,128)(2,1)S(1)} collective-permute-done((bf16[96,1024]{1,0:T(8,128)(2,1)S(1)}, bf16[96,1024]{1,0:T(8,128)(2,1)S(1)}, u32[]{:S(2)}, u32[]{:S(2)}) %collective-permute-start.6) | collective-permute-done | bytes 196640 | tf_op jit(solution)/shard_map/ppermute | solution.py:27
  152.3 2.6 %collective-permute-start.31 = (bf16[96,2048]{1,0:T(8,128)(2,1)}, bf16[96,2048]{1,0:T(8,128)(2,1)}, u32[]{:S(2)}, u32[]{:S(2)}) collective-permute-start(bf16[96,2048]{1,0:T(8,128)(2,1)} %get-tuple-element.60), channel_id=1, source_target_pairs={{0,12},{4,8},{8,4},{12,0},{16,28},{20,24},{24,20},{28,16},{1,13},{... | collective-permute-start | bytes 1179656 | tf_op jit(solution)/shard_map/ppermute | solution.py:27
  154.9 5.6 %expert_far.1 = (bf16[96,2048]{1,0:T(8,128)(2,1)S(1)}, bf16[96,2048]{1,0:T(8,128)(2,1)}, bf16[96,2048]{1,0:T(8,128)(2,1)}, bf16[96,2048]{1,0:T(8,128)(2,1)}) custom-call(f32[1,2048]{1,0:T(1,128)S(1)} %bitcast.5, bf16[192,1024]{1,0:T(8,128)(2,1)S(1)} %get-tuple-element.38.refs_0_, bf16[96,1024]{1,0:T(8,128)(2,1)S(1)} %get-tuple-element.39.refs_1_, ...), custom_call_target="tpu_custom_call" | custom-call | tf_op jit(solution)/shard_map/expert_far/pallas_call | solution.py:257
  160.5 0.8 copy-done.9
  161.3 0.6 collective-permute-start.23
  162.2 2.6 %collective-permute-start.25 = (bf16[96,2048]{1,0:T(8,128)(2,1)}, bf16[96,2048]{1,0:T(8,128)(2,1)S(1)}, u32[]{:S(2)}, u32[]{:S(2)}) collective-permute-start(bf16[96,2048]{1,0:T(8,128)(2,1)} %get-tuple-element.52), channel_id=1, source_target_pairs={{0,12},{4,8},{8,4},{12,0},{16,28},{20,24},{24,20},{28,16},{1,13},{... | collective-permute-start | bytes 1179656 | tf_op jit(solution)/shard_map/ppermute | solution.py:27
  165.2 2.6 %combine.2.refs_4_ = f32[256,2048]{1,0:T(8,128)S(1)} custom-call(s32[256,2]{1,0:T(8,128)S(1)} %copy.19.slots_ref, f32[256,2]{1,0:T(8,128)S(1)} %broadcast_divide_fusion.share_ref, bf16[96,2048]{1,0:T(8,128)(2,1)S(1)} %get-tuple-element.57.refs_0_, bf16[96,2048]{1,0:T(8,128)(2,1)S(1)} %collective-permute-done.29.refs_1_, ...), custom_call_target="tpu_custom_call" | custom-call | tf_op jit(solution)/shard_map/combine/pallas_call | solution.py:299
  167.8 6.1 %collective-permute-done.23.refs_1_ = bf16[96,2048]{1,0:T(8,128)(2,1)S(1)} collective-permute-done((bf16[96,2048]{1,0:T(8,128)(2,1)}, bf16[96,2048]{1,0:T(8,128)(2,1)S(1)}, u32[]{:S(2)}, u32[]{:S(2)}) %collective-permute-start.23) | collective-permute-done | bytes 393248 | tf_op jit(solution)/shard_map/ppermute | solution.py:27
  174.1 7.5 %collective-permute-done.25.refs_3_ = bf16[96,2048]{1,0:T(8,128)(2,1)S(1)} collective-permute-done((bf16[96,2048]{1,0:T(8,128)(2,1)}, bf16[96,2048]{1,0:T(8,128)(2,1)S(1)}, u32[]{:S(2)}, u32[]{:S(2)}) %collective-permute-start.25) | collective-permute-done | bytes 393248 | tf_op jit(solution)/shard_map/ppermute | solution.py:27
  181.6 2.4 %combine.3 = bf16[256,2048]{1,0:T(8,128)(2,1)} custom-call(s32[256,2]{1,0:T(8,128)S(1)} %copy.19.slots_ref, f32[256,2]{1,0:T(8,128)S(1)} %broadcast_divide_fusion.share_ref, bf16[96,2048]{1,0:T(8,128)(2,1)S(1)} %copy-done.10, bf16[96,2048]{1,0:T(8,128)(2,1)S(1)} %collective-permute-done.23.refs_1_, bf16[96,2048]{1,0:T(8,128)(2,1)S(1)} %collective-permute-done.24.refs_2_, ...), custom_call_target="tpu_custom_call" | custom-call | tf_op jit(solution)/shard_map/combine/pallas_call | solution.py:299
  (66 shorter events, 1.6 us)
Async XLA Ops:
  0.0 9.3 %copy-start.5 = (bf16[1024,512]{1,0:T(8,128)(2,1)S(1)}, bf16[1024,512]{1,0:T(8,128)(2,1)}, u32[]{:S(2)}) copy-start(bf16[1024,512]{1,0:T(8,128)(2,1)} %x_ref.3) | copy-start | bytes 3145732
  0.0 9.3 %copy-start.12 = (f32[512]{0:T(512)S(1)}, f32[512]{0:T(512)}, u32[]{:S(2)}) copy-start(f32[512]{0:T(512)} %param.13) | copy-start | bytes 6148
  0.0 21.1 %collective-permute-start.2 = (bf16[512,2048]{1,0:T(8,128)(2,1)}, bf16[512,2048]{1,0:T(8,128)(2,1)}, u32[]{:S(2)}, u32[]{:S(2)}) collective-permute-start(bf16[512,2048]{1,0:T(8,128)(2,1)} %refs_2_.7), channel_id=1, source_target_pairs={{0,1},{1,0},{2,3},{3,2},{4,5},{5,4},{6,7},{7,6},{8,9},{9,8},{10,11... | collective-permute-start | bytes 6291464 | tf_op jit(solution)/shard_map/ppermute | solution.py:27
  0.5 20.6 %copy-start = (bf16[512,2048]{1,0:T(8,128)(2,1)S(1)}, bf16[512,2048]{1,0:T(8,128)(2,1)}, u32[]{:S(2)}) copy-start(bf16[512,2048]{1,0:T(8,128)(2,1)} %refs_2_.7) | copy-start | bytes 6291460
  3.2 6.1 %collective-permute-start = (bf16[16,512]{1,0:T(8,128)(2,1)}, bf16[16,512]{1,0:T(8,128)(2,1)S(1)}, u32[]{:S(2)}, u32[]{:S(2)}) collective-permute-start(bf16[16,512]{1,0:T(8,128)(2,1)} %get-tuple-element.34), channel_id=1, source_target_pairs={{0,4},{4,8},{8,12},{12,16},{16,20},{20,24},{24,28},{1,5},{5,9},{9,... | collective-permute-start | bytes 49160 | tf_op jit(solution)/shard_map/ppermute | solution.py:112
  9.3 1.0 copy-start.8
  11.9 12.1 %copy-start.6 = (bf16[256,512]{1,0:T(8,128)(2,1)}, bf16[256,512]{1,0:T(8,128)(2,1)S(1)}, u32[]{:S(2)}) copy-start(bf16[256,512]{1,0:T(8,128)(2,1)S(1)} %get-tuple-element.37.refs_0_) | copy-start | bytes 786436
  11.9 9.2 %collective-permute-start.1 = (bf16[512,512]{1,0:T(8,128)(2,1)S(1)}, bf16[512,512]{1,0:T(8,128)(2,1)S(1)}, u32[]{:S(2)}, u32[]{:S(2)}) collective-permute-start(bf16[512,512]{1,0:T(8,128)(2,1)S(1)} %get-tuple-element.36), channel_id=1, source_target_pairs={{0,1},{1,0},{2,3},{3,2},{4,5},{5,4},{6,7},{7,6},{8,9},{9,8},{10,11... | collective-permute-start | bytes 1572872 | tf_op jit(solution)/shard_map/ppermute | solution.py:27
  12.0 18.4 %collective-permute-start.11 = (bf16[512,512]{1,0:T(8,128)(2,1)}, bf16[512,512]{1,0:T(8,128)(2,1)S(1)}, u32[]{:S(2)}, u32[]{:S(2)}) collective-permute-start(bf16[512,512]{1,0:T(8,128)(2,1)} %get-tuple-element.46), channel_id=1, source_target_pairs={{0,24},{4,28},{8,16},{12,20},{16,8},{20,12},{24,0},{28,4},{1,25},{... | collective-permute-start | bytes 1572872 | tf_op jit(solution)/shard_map/ppermute | solution.py:338
  17.3 24.4 %collective-permute-start.12 = (bf16[512,512]{1,0:T(8,128)(2,1)}, bf16[512,512]{1,0:T(8,128)(2,1)}, u32[]{:S(2)}, u32[]{:S(2)}) collective-permute-start(bf16[512,512]{1,0:T(8,128)(2,1)} %get-tuple-element.47), channel_id=1, source_target_pairs={{0,24},{4,28},{8,16},{12,20},{16,8},{20,12},{24,0},{28,4},{1,25},{... | collective-permute-start | bytes 1572872 | tf_op jit(solution)/shard_map/ppermute | solution.py:338
  17.4 35.3 %collective-permute-start.13 = (bf16[512,512]{1,0:T(8,128)(2,1)}, bf16[512,512]{1,0:T(8,128)(2,1)}, u32[]{:S(2)}, u32[]{:S(2)}) collective-permute-start(bf16[512,512]{1,0:T(8,128)(2,1)} %get-tuple-element.48), channel_id=1, source_target_pairs={{0,24},{4,28},{8,16},{12,20},{16,8},{20,12},{24,0},{28,4},{1,25},{... | collective-permute-start | bytes 1572872 | tf_op jit(solution)/shard_map/ppermute | solution.py:338
  23.9 30.3 %collective-permute-start.4 = (bf16[256,1024]{1,0:T(8,128)(2,1)}, bf16[256,1024]{1,0:T(8,128)(2,1)}, u32[]{:S(2)}, u32[]{:S(2)}) collective-permute-start(bf16[256,1024]{1,0:T(8,128)(2,1)} %project.7), channel_id=1, source_target_pairs={{0,2},{1,3},{2,0},{3,1},{4,6},{5,7},{6,4},{7,5},{8,10},{9,11},{10,... | collective-permute-start | bytes 1572872 | tf_op jit(solution)/shard_map/ppermute | solution.py:27
  25.4 28.8 %copy-start.14 = (s32[256,2]{0,1:T(2,128)S(1)}, s32[256,2]{0,1:T(2,128)}, u32[]{:S(2)}) copy-start(s32[256,2]{0,1:T(2,128)} %param.20) | copy-start | bytes 6148
  25.4 29.6 %copy-start.4 = (bf16[256,2048]{1,0:T(8,128)(2,1)S(1)}, bf16[256,2048]{1,0:T(8,128)(2,1)}, u32[]{:S(2)}) copy-start(bf16[256,2048]{1,0:T(8,128)(2,1)} %refs_4_.3) | copy-start | bytes 3145732
  30.4 43.5 %collective-permute-start.14 = (bf16[512,512]{1,0:T(8,128)(2,1)S(1)}, bf16[512,512]{1,0:T(8,128)(2,1)S(1)}, u32[]{:S(2)}, u32[]{:S(2)}) collective-permute-start(bf16[512,512]{1,0:T(8,128)(2,1)S(1)} %collective-permute-done.11.refs_8_), channel_id=1, source_target_pairs={{0,1},{1,0},{2,3},{3,2},{4,5},{5,4},{6,7},{7,6},{8,9},{9,8},{10,11... | collective-permute-start | bytes 1572872 | tf_op jit(solution)/shard_map/ppermute | solution.py:27
  30.4 45.0 %collective-permute-start.17 = (bf16[512,512]{1,0:T(8,128)(2,1)S(1)}, bf16[512,512]{1,0:T(8,128)(2,1)S(1)}, u32[]{:S(2)}, u32[]{:S(2)}) collective-permute-start(bf16[512,512]{1,0:T(8,128)(2,1)S(1)} %collective-permute-done.11.refs_8_), channel_id=1, source_target_pairs={{0,2},{1,3},{2,0},{3,1},{4,6},{5,7},{6,4},{7,5},{8,10},{9,11},{10,... | collective-permute-start | bytes 1572872 | tf_op jit(solution)/shard_map/ppermute | solution.py:27
  41.7 62.6 %collective-permute-start.18 = (bf16[512,512]{1,0:T(8,128)(2,1)}, bf16[512,512]{1,0:T(8,128)(2,1)S(1)}, u32[]{:S(2)}, u32[]{:S(2)}) collective-permute-start(bf16[512,512]{1,0:T(8,128)(2,1)} %collective-permute-done.12.refs_9_), channel_id=1, source_target_pairs={{0,2},{1,3},{2,0},{3,1},{4,6},{5,7},{6,4},{7,5},{8,10},{9,11},{10,... | collective-permute-start | bytes 1572872 | tf_op jit(solution)/shard_map/ppermute | solution.py:27
  43.2 0.9 copy-start.7
  52.7 19.9 %collective-permute-start.3 = (bf16[256,1024]{1,0:T(8,128)(2,1)S(1)}, bf16[256,1024]{1,0:T(8,128)(2,1)S(1)}, u32[]{:S(2)}, u32[]{:S(2)}) collective-permute-start(bf16[256,1024]{1,0:T(8,128)(2,1)S(1)} %project.5), channel_id=1, source_target_pairs={{0,2},{1,3},{2,0},{3,1},{4,6},{5,7},{6,4},{7,5},{8,10},{9,11},{10,... | collective-permute-start | bytes 1572872 | tf_op jit(solution)/shard_map/ppermute | solution.py:27
  54.2 50.2 %collective-permute-start.19 = (bf16[512,512]{1,0:T(8,128)(2,1)}, bf16[512,512]{1,0:T(8,128)(2,1)S(1)}, u32[]{:S(2)}, u32[]{:S(2)}) collective-permute-start(bf16[512,512]{1,0:T(8,128)(2,1)} %collective-permute-done.13.refs_10_), channel_id=1, source_target_pairs={{0,2},{1,3},{2,0},{3,1},{4,6},{5,7},{6,4},{7,5},{8,10},{9,11},{10,... | collective-permute-start | bytes 1572872 | tf_op jit(solution)/shard_map/ppermute | solution.py:27
  57.2 71.3 %copy-start.2 = (bf16[1,2048,512]{2,1,0:T(8,128)(2,1)S(1)}, bf16[1,2048,512]{2,1,0:T(8,128)(2,1)}, u32[]{:S(2)}) copy-start(bf16[1,2048,512]{2,1,0:T(8,128)(2,1)} %refs_9_.1) | copy-start | bytes 6291460
  57.2 71.3 %copy-start.3 = (bf16[1,512,2048]{2,1,0:T(8,128)(2,1)S(1)}, bf16[1,512,2048]{2,1,0:T(8,128)(2,1)}, u32[]{:S(2)}) copy-start(bf16[1,512,2048]{2,1,0:T(8,128)(2,1)} %refs_10_.1) | copy-start | bytes 6291460
  59.5 69.1 %copy-start.1 = (bf16[1,2048,512]{2,1,0:T(8,128)(2,1)S(1)}, bf16[1,2048,512]{2,1,0:T(8,128)(2,1)}, u32[]{:S(2)}) copy-start(bf16[1,2048,512]{2,1,0:T(8,128)(2,1)} %refs_8_.1) | copy-start | bytes 6291460
  59.5 69.1 %copy-start.11 = (f32[2048]{0:T(1024)S(1)}, f32[2048]{0:T(1024)}, u32[]{:S(2)}) copy-start(f32[2048]{0:T(1024)} %param.16) | copy-start | bytes 24580
  72.7 39.5 %collective-permute-start.26 = (bf16[96,1024]{1,0:T(8,128)(2,1)S(1)}, bf16[96,1024]{1,0:T(8,128)(2,1)S(1)}, u32[]{:S(2)}, u32[]{:S(2)}) collective-permute-start(bf16[96,1024]{1,0:T(8,128)(2,1)S(1)} %get-tuple-element.54), channel_id=1, source_target_pairs={{0,4},{4,0},{8,12},{12,8},{16,20},{20,16},{24,28},{28,24},{1,5},{5... | collective-permute-start | bytes 589832 | tf_op jit(solution)/shard_map/ppermute | solution.py:27
  73.9 48.9 %collective-permute-start.5 = (bf16[192,1024]{1,0:T(8,128)(2,1)S(1)}, bf16[192,1024]{1,0:T(8,128)(2,1)S(1)}, u32[]{:S(2)}, u32[]{:S(2)}) collective-permute-start(bf16[192,1024]{1,0:T(8,128)(2,1)S(1)} %get-tuple-element.40), channel_id=1, source_target_pairs={{0,4},{4,0},{8,12},{12,8},{16,20},{20,16},{24,28},{28,24},{1,5},{5... | collective-permute-start | bytes 1179656 | tf_op jit(solution)/shard_map/ppermute | solution.py:27
  75.4 47.9 %collective-permute-start.7 = (bf16[192,1024]{1,0:T(8,128)(2,1)S(1)}, bf16[192,1024]{1,0:T(8,128)(2,1)S(1)}, u32[]{:S(2)}, u32[]{:S(2)}) collective-permute-start(bf16[192,1024]{1,0:T(8,128)(2,1)S(1)} %get-tuple-element.42), channel_id=1, source_target_pairs={{0,8},{4,12},{8,0},{12,4},{16,24},{20,28},{24,16},{28,20},{1,9},{5... | collective-permute-start | bytes 1179656 | tf_op jit(solution)/shard_map/ppermute | solution.py:27
  104.3 14.2 %collective-permute-start.27 = (bf16[96,1024]{1,0:T(8,128)(2,1)S(1)}, bf16[96,1024]{1,0:T(8,128)(2,1)S(1)}, u32[]{:S(2)}, u32[]{:S(2)}) collective-permute-start(bf16[96,1024]{1,0:T(8,128)(2,1)S(1)} %get-tuple-element.55), channel_id=1, source_target_pairs={{0,8},{4,12},{8,0},{12,4},{16,24},{20,28},{24,16},{28,20},{1,9},{5... | collective-permute-start | bytes 589832 | tf_op jit(solution)/shard_map/ppermute | solution.py:27
  104.4 18.4 %collective-permute-start.28 = (bf16[96,1024]{1,0:T(8,128)(2,1)S(1)}, bf16[96,1024]{1,0:T(8,128)(2,1)S(1)}, u32[]{:S(2)}, u32[]{:S(2)}) collective-permute-start(bf16[96,1024]{1,0:T(8,128)(2,1)S(1)} %get-tuple-element.56), channel_id=1, source_target_pairs={{0,12},{4,8},{8,4},{12,0},{16,28},{20,24},{24,20},{28,16},{1,13},{... | collective-permute-start | bytes 589832 | tf_op jit(solution)/shard_map/ppermute | solution.py:27
  112.1 16.4 %collective-permute-start.9 = (bf16[192,1024]{1,0:T(8,128)(2,1)S(1)}, bf16[192,1024]{1,0:T(8,128)(2,1)S(1)}, u32[]{:S(2)}, u32[]{:S(2)}) collective-permute-start(bf16[192,1024]{1,0:T(8,128)(2,1)S(1)} %get-tuple-element.44), channel_id=1, source_target_pairs={{0,12},{4,8},{8,4},{12,0},{16,28},{20,24},{24,20},{28,16},{1,13},{... | collective-permute-start | bytes 1179656 | tf_op jit(solution)/shard_map/ppermute | solution.py:27
  118.5 13.9 %collective-permute-start.15 = (bf16[512,512]{1,0:T(8,128)(2,1)}, bf16[512,512]{1,0:T(8,128)(2,1)S(1)}, u32[]{:S(2)}, u32[]{:S(2)}) collective-permute-start(bf16[512,512]{1,0:T(8,128)(2,1)} %collective-permute-done.12.refs_9_), channel_id=1, source_target_pairs={{0,1},{1,0},{2,3},{3,2},{4,5},{5,4},{6,7},{7,6},{8,9},{9,8},{10,11... | collective-permute-start | bytes 1572872 | tf_op jit(solution)/shard_map/ppermute | solution.py:27
  122.8 11.0 %collective-permute-start.16 = (bf16[512,512]{1,0:T(8,128)(2,1)}, bf16[512,512]{1,0:T(8,128)(2,1)S(1)}, u32[]{:S(2)}, u32[]{:S(2)}) collective-permute-start(bf16[512,512]{1,0:T(8,128)(2,1)} %collective-permute-done.13.refs_10_), channel_id=1, source_target_pairs={{0,1},{1,0},{2,3},{3,2},{4,5},{5,4},{6,7},{7,6},{8,9},{9,8},{10,11... | collective-permute-start | bytes 1572872 | tf_op jit(solution)/shard_map/ppermute | solution.py:27
  122.8 11.6 %collective-permute-start.20 = (bf16[512,512]{1,0:T(8,128)(2,1)S(1)}, bf16[512,512]{1,0:T(8,128)(2,1)S(1)}, u32[]{:S(2)}, u32[]{:S(2)}) collective-permute-start(bf16[512,512]{1,0:T(8,128)(2,1)S(1)} %collective-permute-done.17.refs_14_), channel_id=1, source_target_pairs={{0,1},{1,0},{2,3},{3,2},{4,5},{5,4},{6,7},{7,6},{8,9},{9,8},{10,11... | collective-permute-start | bytes 1572872 | tf_op jit(solution)/shard_map/ppermute | solution.py:27
  123.3 12.9 %collective-permute-start.21 = (bf16[512,512]{1,0:T(8,128)(2,1)S(1)}, bf16[512,512]{1,0:T(8,128)(2,1)S(1)}, u32[]{:S(2)}, u32[]{:S(2)}) collective-permute-start(bf16[512,512]{1,0:T(8,128)(2,1)S(1)} %collective-permute-done.18.refs_15_), channel_id=1, source_target_pairs={{0,1},{1,0},{2,3},{3,2},{4,5},{5,4},{6,7},{7,6},{8,9},{9,8},{10,11... | collective-permute-start | bytes 1572872 | tf_op jit(solution)/shard_map/ppermute | solution.py:27
  128.5 8.8 %collective-permute-start.22 = (bf16[512,512]{1,0:T(8,128)(2,1)S(1)}, bf16[512,512]{1,0:T(8,128)(2,1)S(1)}, u32[]{:S(2)}, u32[]{:S(2)}) collective-permute-start(bf16[512,512]{1,0:T(8,128)(2,1)S(1)} %collective-permute-done.19.refs_16_), channel_id=1, source_target_pairs={{0,1},{1,0},{2,3},{3,2},{4,5},{5,4},{6,7},{7,6},{8,9},{9,8},{10,11... | collective-permute-start | bytes 1572872 | tf_op jit(solution)/shard_map/ppermute | solution.py:27
  132.4 29.8 %collective-permute-start.29 = (bf16[96,2048]{1,0:T(8,128)(2,1)S(1)}, bf16[96,2048]{1,0:T(8,128)(2,1)S(1)}, u32[]{:S(2)}, u32[]{:S(2)}) collective-permute-start(bf16[96,2048]{1,0:T(8,128)(2,1)S(1)} %get-tuple-element.58), channel_id=1, source_target_pairs={{0,4},{4,0},{8,12},{12,8},{16,20},{20,16},{24,28},{28,24},{1,5},{5... | collective-permute-start | bytes 1179656 | tf_op jit(solution)/shard_map/ppermute | solution.py:27
  133.8 18.5 %collective-permute-start.6 = (bf16[96,1024]{1,0:T(8,128)(2,1)S(1)}, bf16[96,1024]{1,0:T(8,128)(2,1)S(1)}, u32[]{:S(2)}, u32[]{:S(2)}) collective-permute-start(bf16[96,1024]{1,0:T(8,128)(2,1)S(1)} %get-tuple-element.41), channel_id=1, source_target_pairs={{0,4},{4,0},{8,12},{12,8},{16,20},{20,16},{24,28},{28,24},{1,5},{5... | collective-permute-start | bytes 589832 | tf_op jit(solution)/shard_map/ppermute | solution.py:27
  134.4 20.5 %collective-permute-start.8 = (bf16[96,1024]{1,0:T(8,128)(2,1)S(1)}, bf16[96,1024]{1,0:T(8,128)(2,1)S(1)}, u32[]{:S(2)}, u32[]{:S(2)}) collective-permute-start(bf16[96,1024]{1,0:T(8,128)(2,1)S(1)} %get-tuple-element.43), channel_id=1, source_target_pairs={{0,8},{4,12},{8,0},{12,4},{16,24},{20,28},{24,16},{28,20},{1,9},{5... | collective-permute-start | bytes 589832 | tf_op jit(solution)/shard_map/ppermute | solution.py:27
  136.1 18.7 %collective-permute-start.10 = (bf16[96,1024]{1,0:T(8,128)(2,1)S(1)}, bf16[96,1024]{1,0:T(8,128)(2,1)S(1)}, u32[]{:S(2)}, u32[]{:S(2)}) collective-permute-start(bf16[96,1024]{1,0:T(8,128)(2,1)S(1)} %get-tuple-element.45), channel_id=1, source_target_pairs={{0,12},{4,8},{8,4},{12,0},{16,28},{20,24},{24,20},{28,16},{1,13},{... | collective-permute-start | bytes 589832 | tf_op jit(solution)/shard_map/ppermute | solution.py:27
  137.3 27.9 %collective-permute-start.30 = (bf16[96,2048]{1,0:T(8,128)(2,1)}, bf16[96,2048]{1,0:T(8,128)(2,1)}, u32[]{:S(2)}, u32[]{:S(2)}) collective-permute-start(bf16[96,2048]{1,0:T(8,128)(2,1)} %get-tuple-element.59), channel_id=1, source_target_pairs={{0,8},{4,12},{8,0},{12,4},{16,24},{20,28},{24,16},{28,20},{1,9},{5... | collective-permute-start | bytes 1179656 | tf_op jit(solution)/shard_map/ppermute | solution.py:27
  152.3 12.9 %collective-permute-start.31 = (bf16[96,2048]{1,0:T(8,128)(2,1)}, bf16[96,2048]{1,0:T(8,128)(2,1)}, u32[]{:S(2)}, u32[]{:S(2)}) collective-permute-start(bf16[96,2048]{1,0:T(8,128)(2,1)} %get-tuple-element.60), channel_id=1, source_target_pairs={{0,12},{4,8},{8,4},{12,0},{16,28},{20,24},{24,20},{28,16},{1,13},{... | collective-permute-start | bytes 1179656 | tf_op jit(solution)/shard_map/ppermute | solution.py:27
  154.9 10.0 %copy-start.13 = (f32[256,2]{0,1:T(2,128)S(1)}, f32[256,2]{0,1:T(2,128)}, u32[]{:S(2)}) copy-start(f32[256,2]{0,1:T(2,128)} %param.21) | copy-start | bytes 6148
  160.5 0.8 copy-start.9
  161.3 12.6 %collective-permute-start.23 = (bf16[96,2048]{1,0:T(8,128)(2,1)}, bf16[96,2048]{1,0:T(8,128)(2,1)S(1)}, u32[]{:S(2)}, u32[]{:S(2)}) collective-permute-start(bf16[96,2048]{1,0:T(8,128)(2,1)} %get-tuple-element.50), channel_id=1, source_target_pairs={{0,4},{4,0},{8,12},{12,8},{16,20},{20,16},{24,28},{28,24},{1,5},{5... | collective-permute-start | bytes 1179656 | tf_op jit(solution)/shard_map/ppermute | solution.py:27
  161.9 12.2 %collective-permute-start.24 = (bf16[96,2048]{1,0:T(8,128)(2,1)}, bf16[96,2048]{1,0:T(8,128)(2,1)S(1)}, u32[]{:S(2)}, u32[]{:S(2)}) collective-permute-start(bf16[96,2048]{1,0:T(8,128)(2,1)} %get-tuple-element.51), channel_id=1, source_target_pairs={{0,8},{4,12},{8,0},{12,4},{16,24},{20,28},{24,16},{28,20},{1,9},{5... | collective-permute-start | bytes 1179656 | tf_op jit(solution)/shard_map/ppermute | solution.py:27
  162.2 19.4 %collective-permute-start.25 = (bf16[96,2048]{1,0:T(8,128)(2,1)}, bf16[96,2048]{1,0:T(8,128)(2,1)S(1)}, u32[]{:S(2)}, u32[]{:S(2)}) collective-permute-start(bf16[96,2048]{1,0:T(8,128)(2,1)} %get-tuple-element.52), channel_id=1, source_target_pairs={{0,12},{4,8},{8,4},{12,0},{16,28},{20,24},{24,20},{28,16},{1,13},{... | collective-permute-start | bytes 1179656 | tf_op jit(solution)/shard_map/ppermute | solution.py:27
  165.2 16.4 %copy-start.10 = (bf16[96,2048]{1,0:T(8,128)(2,1)S(1)}, bf16[96,2048]{1,0:T(8,128)(2,1)}, u32[]{:S(2)}) copy-start(bf16[96,2048]{1,0:T(8,128)(2,1)} %copy-done.9) | copy-start | bytes 1179652
